TPU v7x, 256 devices: a whole 4x4x8 slice. The times are simulated.
256 devices in a mesh: sp: 64 (over z, x, core), tp: 4 (over y).
Axes of the slice: x: 4, y: 4, z: 8, core: 2. Of those that a mesh axis runs over, the one named last changes fastest.
Arguments:
- stream: bfloat16 [8192, 2048], P(('sp', 'tp')), may hold values from -2.5 to 2.5
- recurrence_input: bfloat16 [8192, 2, 1024], P('sp', None, 'tp'), may hold values from -6 to 6
- output_gate_input: bfloat16 [8192, 2, 1024], P('sp', None, 'tp'), may hold values from -6 to 6
- convolution_taps: bfloat16 [4, 2, 1024], P(None, None, 'tp'), may hold values from -4 to 4
- first_group_gates: bfloat16 [2, 16, 64, 64], P(None, 'tp'), may hold values from -0.75 to 0.75
- second_group_gates: bfloat16 [2, 8, 128, 128], P(None, 'tp'), may hold values from -0.5 to 0.5
- channel_decay: float32 [2, 1024], P(None, 'tp'), may hold values from 4.7 to 13.6
- position_log_extra: float32 [8192, 2, 1024], P('sp', None, 'tp'), may hold values from -1.4 to 0, as said below
- recurrence_output_weight: bfloat16 [2, 1024, 2048], P(None, 'tp'), may hold values from -0.125 to 0.125
- first_norm_gain: float32 [2048], replicated, may hold values from 0.1 to 1.9
- first_norm_bias: float32 [2048], replicated, may hold values from -1.75 to 1.75
- routed_expert_index: int32 [8192, 4], P('sp'), may hold values from 0 to 63, all different within a row; in each aligned block of 32 rows (0 to 31, 32 to 63, ...) at most 2 rows name the same one
- routed_expert_weight: float32 [8192, 4], P('sp'), may hold values from 0.25 to 1
- routed_gate_weight: bfloat16 [64, 2048, 512], P('sp', None, 'tp'), may hold values from -0.125 to 0.125
- routed_up_weight: bfloat16 [64, 2048, 512], P('sp', None, 'tp'), may hold values from -0.125 to 0.125
- routed_down_weight: bfloat16 [64, 512, 2048], P('sp', 'tp'), may hold values from -0.25 to 0.25
- shared_gate_weight: bfloat16 [2048, 512], replicated, may hold values from -0.125 to 0.125
- shared_up_weight: bfloat16 [2048, 512], replicated, may hold values from -0.125 to 0.125
- shared_down_weight: bfloat16 [512, 2048], replicated, may hold values from -0.25 to 0.25
- second_norm_gain: float32 [2048], replicated, may hold values from 0.1 to 1.9
- second_norm_bias: float32 [2048], replicated, may hold values from -1.75 to 1.75
Outputs:
- result: bfloat16 [8192, 2048], P(('sp', 'tp'))
Inputs may be any that keep to these rules, and one draw needn't show every extreme that they name: `routed_expert_index`: each row names 4 different experts. In each aligned block of 32 rows no expert is named more than 2 times, and in some block an expert is named exactly 2 times. `position_log_extra`: every entry is negative.
All inputs are finite; a program needn't handle non-finite values.
Results may differ from a plain program's by a relative error of at most 0.015.
Values may be sent and summed in bfloat16 or wider, within the bound.
No kernel may reach another device: no remote copies, remote signals or barrier semaphores. Data moves between devices by JAX's collectives and lax.ppermute only.
A program may use at most 64 MiB of HBM per device.

v0:
```python
import jax
import jax.numpy as jnp
from jax import lax
from jax.experimental import pallas as pl
from jax.experimental.pallas import tpu as pltpu
from jax.sharding import PartitionSpec as P

RESIDUAL_SCALE = 8.0**0.25
NORM_EPSILON = 1e-05
LANES = 128
SLOTS = 2
BF16, F32 = jnp.bfloat16, jnp.float32
VMEM = pl.BlockSpec(memory_space=pltpu.VMEM)
SMEM = pl.BlockSpec(memory_space=pltpu.SMEM)
ANY = pl.BlockSpec(memory_space=pl.ANY)


def kernel_call(body, out_shape, *operands, scratch=(), limit=16):
    several = isinstance(out_shape, (list, tuple))
    specs, arrays = [], []
    for operand in operands:
        array, place = operand if isinstance(operand, tuple) else (operand, None)
        specs.append({"smem": SMEM, "hbm": ANY}.get(place, VMEM))
        if place != "smem":
            array = pltpu.with_memory_space_constraint(array, pltpu.VMEM if place == "vmem" else pltpu.HBM)
        arrays.append(array)
    return pl.pallas_call(
        body,
        out_shape=out_shape,
        in_specs=specs,
        out_specs=[VMEM] * len(out_shape) if several else VMEM,
        scratch_shapes=scratch,
        compiler_params=pltpu.CompilerParams(vmem_limit_bytes=limit << 20),
    )(*arrays)


def fetched(pairs, sems):
    copies = [pltpu.make_async_copy(source, target, sems.at[k]) for k, (source, target) in enumerate(pairs)]
    for copy in copies:
        copy.start()
    return copies


def dot(a, b):
    return jnp.dot(a, b, preferred_element_type=F32)


def layer_norm(values, gain_vec, bias_vec):
    row_mean = jnp.mean(values, axis=-1, keepdims=True)
    spread = jnp.mean(jnp.square(values - row_mean), axis=-1, keepdims=True)
    return (values - row_mean) * lax.rsqrt(spread + NORM_EPSILON) * gain_vec + bias_vec


def softplus(x):
    u = jnp.exp(-jnp.abs(x))
    s = u / (2.0 + u)
    q = s * s
    series = 1.0 / 17.0
    for k in (15.0, 13.0, 11.0, 9.0, 7.0, 5.0, 3.0, 1.0):
        series = series * q + 1.0 / k
    return jnp.maximum(x, 0.0) + 2.0 * s * series


def expm1(z):
    series = 1.0 + z * (1.0 / 9.0)
    for k in (8.0, 7.0, 6.0, 5.0, 4.0, 3.0, 2.0):
        series = 1.0 + z * (1.0 / k) * series
    return jnp.where(jnp.abs(z) < 0.5, z * series, jnp.exp(z) - 1.0)


def shifted_rows(values, by, row, fill):
    if by < 8:
        return jnp.where(row >= by, pltpu.roll(values, by, 0), fill)
    head = jnp.full((by, values.shape[1]), fill, values.dtype)
    return jnp.concatenate([head, values[: values.shape[0] - by]], axis=0)


def chain_rows(decay, drive):
    row = lax.broadcasted_iota(jnp.int32, decay.shape, 0)
    by = 1
    while by < decay.shape[0]:
        drive = decay * shifted_rows(drive, by, row, 0.0) + drive
        decay = decay * shifted_rows(decay, by, row, 1.0)
        by *= 2
    return decay, drive


def flat(array):
    length, groups, half = array.shape
    return array.reshape(length, groups, half // LANES, LANES).transpose(0, 2, 1, 3).reshape(-1, LANES)


def local_kernel(rows, border, taps, small_maps, large_maps, decay_param, extra, decays, states, totals, padded, maps):
    groups, half = decay_param.shape
    per_half = half // LANES
    step = groups * per_half
    length = rows.shape[0] // step
    tap_count = taps.shape[0]
    tap_weights = taps[...].astype(F32)
    rate = -8.0 * softplus(-decay_param[...])
    margin = border.shape[0]
    padded[0:margin] = border[...].astype(F32)
    padded[margin:] = rows[...].astype(F32)
    logs, ends = [], []
    for g, blocks in enumerate((small_maps, large_maps)):
        conv_runs = []
        for c in range(per_half):
            at = slice(c * LANES, (c + 1) * LANES)
            summed = None
            for k in range(tap_count):
                start = margin - (tap_count - 1 - k) * step + c * groups + g
                term = tap_weights[k, g : g + 1, at] * padded[pl.ds(start, length, stride=step), :]
                summed = term if summed is None else summed + term
            conv_runs.append(summed.astype(BF16))
        conv_rows = jnp.concatenate(conv_runs, axis=1)
        maps[...] = jnp.zeros(maps.shape, BF16)
        head = blocks.shape[-1]
        for m in range(2):
            for h in range(blocks.shape[1]):
                maps[h * head : (h + 1) * head, m * half + h * head : m * half + (h + 1) * head] = blocks[m, h]
        gates = jax.nn.sigmoid(dot(conv_rows, maps[...]))
        for c in range(per_half):
            at = slice(c * LANES, (c + 1) * LANES)
            log_decay = gates[:, at] * rate[g : g + 1, at] + extra[pl.ds(c * groups + g, length, stride=step), :]
            gate = gates[:, half + c * LANES : half + (c + 1) * LANES]
            drive = jnp.sqrt(-expm1(2.0 * log_decay)) * gate * conv_runs[c].astype(F32)
            product, state = chain_rows(jnp.exp(log_decay), drive)
            to = slice((g * per_half + c) * LANES, (g * per_half + c + 1) * LANES)
            decays[:, to] = product
            states[:, to] = state
            logs.append(jnp.sum(log_decay, axis=0, keepdims=True))
            ends.append(state[length - 1 :])
    span = jnp.concatenate(logs + ends, axis=0).astype(BF16)
    for j in range(totals.shape[0]):
        totals[j] = span


def entering_state(spans, ahead):
    half = spans.shape[1] // 2
    passed = (ahead[...] > 0.0)[:, None, :]
    decays = jnp.where(passed, jnp.exp(spans[:, :half].astype(F32)), 1.0)
    ends = jnp.where(passed, spans[:, half:].astype(F32), 0.0)
    state = ends[0]
    for j in range(1, spans.shape[0] - 1):
        state = decays[j] * state + ends[j]
    return state


def project_kernel(spans, ahead, decays, states, weight, *outs):
    entering = entering_state(spans, ahead)
    runs = entering.shape[0]
    branches = []
    for run in range(runs):
        at = slice(run * LANES, (run + 1) * LANES)
        branches.append((states[:, at] + decays[:, at] * entering[run : run + 1]).astype(BF16))
    acc, per_half = None, runs // weight.shape[0]
    for g in range(weight.shape[0]):
        part = dot(jnp.concatenate(branches[g * per_half : (g + 1) * per_half], axis=1), weight[g])
        acc = part if acc is None else acc + part
    quarter = outs[0].shape[0]
    for k, out in enumerate(outs):
        out[...] = acc[k * quarter : (k + 1) * quarter].astype(BF16)


def route(ids, weights, select, merge, part):
    slot_count, rows = select.shape[0], ids.shape[1]
    kept_rows = select.shape[1]
    turn = (rows - part * kept_rows) % rows
    own = lax.broadcasted_iota(jnp.int32, ids.shape, 1) < kept_rows
    ids = jnp.where(own, pltpu.roll(ids[...], turn, 1), -1)
    weights = pltpu.roll(weights[...], turn, 1)
    slot = lax.broadcasted_iota(jnp.int32, (slot_count, rows), 0)
    names = jnp.zeros((slot_count, rows), F32)
    weight = jnp.zeros((slot_count, rows), F32)
    for k in range(ids.shape[0]):
        named = ids[k : k + 1] == slot // SLOTS
        names = jnp.where(named, 1.0, names)
        weight = jnp.where(named, weights[k : k + 1], weight)
    earlier = lax.broadcasted_iota(jnp.int32, (rows, rows), 0) < lax.broadcasted_iota(jnp.int32, (rows, rows), 1)
    rank = dot(names.astype(BF16), jnp.where(earlier, 1.0, 0.0).astype(BF16))
    taken = (names > 0.0) & (rank == (slot % SLOTS).astype(F32))
    select[...] = jnp.where(taken, 1.0, 0.0).astype(BF16)[:, : select.shape[1]]
    merge[...] = jnp.where(taken, weight, 0.0).T[: merge.shape[0]]


def mix_kernel(*refs):
    *parts, stream, gain, bias, select, normed, outgoing = refs
    mixed = parts[0][...].astype(F32)
    for part in parts[1:]:
        mixed = mixed + part[...].astype(F32)
    rows = layer_norm(RESIDUAL_SCALE * stream[...].astype(F32) + mixed, gain[...], bias[...]).astype(BF16)
    normed[...] = rows
    outgoing[...] = dot(select[...], rows).astype(BF16).reshape(outgoing.shape)


def side_kernel(places, decays, states, *rest):
    *far, select, merge, turned_decays, turned_states, stream, gain, bias, projection, ahead = rest[:16]
    ids, weights, gate_rows, wide, products, sums, sems = rest[16:]
    copies = fetched(list(zip(far, (gate_rows, ids, weights, stream, gain, bias, projection))), sems)
    part, mine = places[0], places[1]
    ahead[...] = jnp.where(lax.broadcasted_iota(jnp.int32, ahead.shape, 0) < mine, 1.0, 0.0)
    length, runs = decays.shape[0], decays.shape[1] // LANES
    copies[0].wait()
    wide[...] = gate_rows[...].astype(F32)
    groups = 2
    for run in range(runs):
        g, c = divmod(run, runs // groups)
        values = jax.nn.gelu(wide[pl.ds(c * groups + g, length, stride=runs), :], approximate=True)
        at = slice(run * LANES, (run + 1) * LANES)
        products[:, at] = values * decays[:, at]
        sums[:, at] = values * states[:, at]
    quarter = stream.shape[0]
    count = length // quarter
    for k in range(count):
        source = pl.ds(pl.multiple_of(lax.rem(part + k, count) * quarter, quarter), quarter)
        turned_decays[k * quarter : (k + 1) * quarter] = products[source]
        turned_states[k * quarter : (k + 1) * quarter] = sums[source]
    copies[1].wait()
    copies[2].wait()
    route(ids, weights, select, merge, part)
    for copy in copies[3:]:
        copy.wait()


def pair_moves(pairs, weights):
    moves = []
    for j, (gate_w, up_w) in enumerate(weights):
        width = gate_w.shape[1]
        moves += [(gate_w, pairs.at[j, :, 0:width]), (up_w, pairs.at[j, :, width : 2 * width])]
    return moves


def shared_kernel(normed, gate_w, up_w, down_w, merge, gain, bias, g0, u0, g1, u1, base, *rest):
    *kept, near, sems = rest
    copies = fetched(pair_moves(near, ((g0, u0), (g1, u1))), sems)
    for target, source in zip(kept, (merge, gain, bias)):
        target[...] = source[...]
    rows = normed[...]
    gated, lifted = dot(rows, gate_w[...]), dot(rows, up_w[...])
    hidden = (jax.nn.silu(gated) * lifted).astype(BF16)
    base[...] = RESIDUAL_SCALE * rows.astype(F32) + dot(hidden, down_w[...])
    for copy in copies:
        copy.wait()


def expert_kernel(rows, near, g2, u2, g3, u3, d0, d1, d2, acc, last, far, down, sems):
    moves = pair_moves(far, ((g2, u2), (g3, u3)))
    unit = d0.shape[0]
    moves += [(piece, down.at[j * unit : (j + 1) * unit]) for j, piece in enumerate((d0, d1, d2))]
    copies = fetched(moves, sems)
    picked = rows[...].reshape(-1, rows.shape[-1])

    def hidden_of(both):
        pair = dot(picked, both)
        return (jax.nn.silu(pair[:, :unit]) * pair[:, unit:]).astype(BF16)

    hidden = [hidden_of(near[j]) for j in range(near.shape[0])]
    for j in range(far.shape[0]):
        copies[2 * j].wait()
        copies[2 * j + 1].wait()
        hidden.append(hidden_of(far[j]))
    last[...] = hidden.pop()
    for copy in copies[2 * far.shape[0] :]:
        copy.wait()
    acc[...] = dot(jnp.concatenate(hidden, axis=1), down[...])


def last_kernel(acc, hidden, d3a, d3b, out):
    total = acc[...] + dot(hidden[...], jnp.concatenate([d3a[...], d3b[...]], axis=0))
    out[...] = total.astype(BF16).reshape(out.shape)


def merge_kernel(returned, base, merge, gain, bias, out):
    rest = merge[...]
    rows = returned[...].reshape(-1, returned.shape[-1])
    total = base[...]
    for _ in range(3):
        part = rest.astype(BF16)
        total = total + dot(part, rows)
        rest = rest - part.astype(F32)
    out[...] = layer_norm(total, gain[...], bias[...]).astype(BF16)


def turned(shard, by):
    count = lax.axis_size("tp")
    return lax.ppermute(shard, "tp", [(i, (i + by) % count) for i in range(count)])


def swapped(pieces, axis):
    return lax.all_to_all(pieces, axis, 0, 0, tiled=True)


def shards(
    stream,
    recurrence_input,
    output_gate_input,
    convolution_taps,
    first_group_gates,
    second_group_gates,
    channel_decay,
    position_log_extra,
    recurrence_output_weight,
    first_norm_gain,
    first_norm_bias,
    routed_expert_index,
    routed_expert_weight,
    routed_gate_weight,
    routed_up_weight,
    routed_down_weight,
    shared_gate_weight,
    shared_up_weight,
    shared_down_weight,
    second_norm_gain,
    second_norm_bias,
):
    length, groups, half = recurrence_input.shape
    width = stream.shape[1]
    tp_count, sp_count = lax.axis_size("tp"), lax.axis_size("sp")
    quarter = length // tp_count
    expert_count = routed_gate_weight.shape[0] * sp_count
    slot_count = expert_count * SLOTS
    channels = groups * half
    shape, kept = jax.ShapeDtypeStruct, pltpu.VMEM

    rows = flat(recurrence_input)
    margin = 16
    border = lax.ppermute(rows[rows.shape[0] - margin :], "sp", [(i, i + 1) for i in range(sp_count - 1)])

    gate_w, up_w, down_w = routed_gate_weight[0], routed_up_weight[0], routed_down_weight[0]
    gate_left, up_right = turned(gate_w, 1), turned(up_w, -1)
    up_left, gate_right = turned(up_w, 1), turned(gate_w, -1)
    down_left, down_right = turned(down_w, 1), turned(down_w, -1)

    runs = channels // LANES
    decays, states, totals = kernel_call(
        local_kernel,
        [kept((length, channels), F32), kept((length, channels), F32), shape((sp_count, 2 * runs, LANES), BF16)],
        rows,
        (border, "vmem"),
        convolution_taps,
        first_group_gates,
        second_group_gates,
        channel_decay,
        flat(position_log_extra),
        scratch=(pltpu.VMEM((margin + rows.shape[0], LANES), F32), pltpu.VMEM((half, 2 * half), BF16)),
    )
    spans = swapped(totals, "sp")

    side = (
        flat(output_gate_input),
        routed_expert_index.T,
        routed_expert_weight.T,
        stream,
        first_norm_gain.reshape(1, width),
        first_norm_bias.reshape(1, width),
        recurrence_output_weight,
    )
    select, merge, decays, states, *norm_parts, projection, ahead = kernel_call(
        side_kernel,
        [
            kept((slot_count, quarter), BF16),
            kept((quarter, slot_count), F32),
            kept((length, channels), F32),
            kept((length, channels), F32),
            kept((quarter, width), BF16),
            kept((1, width), F32),
            kept((1, width), F32),
            kept(recurrence_output_weight.shape, BF16),
            kept((sp_count, LANES), F32),
        ],
        (jnp.stack([lax.axis_index("tp"), lax.axis_index("sp")]), "smem"),
        (decays, "vmem"),
        (states, "vmem"),
        *((x, "hbm") for x in side),
        scratch=(
            pltpu.VMEM(routed_expert_index.T.shape, jnp.int32),
            pltpu.VMEM(routed_expert_weight.T.shape, F32),
            pltpu.VMEM(rows.shape, BF16),
            pltpu.VMEM(rows.shape, F32),
            pltpu.VMEM((length, channels), F32),
            pltpu.VMEM((length, channels), F32),
            pltpu.SemaphoreType.DMA((len(side),)),
        ),
    )
    own, *others = kernel_call(
        project_kernel,
        [kept((quarter, width), BF16) for _ in range(tp_count)],
        *((x, "vmem") for x in (spans, ahead, decays, states, projection)),
    )
    parts = {k: turned(others[k - 1], k) for k in (2, 1, 3)}
    parts = [own, *(parts[k] for k in (1, 3, 2))]

    gate_far, up_far = turned(gate_left, 1), turned(up_right, -1)

    normed, outgoing = kernel_call(
        mix_kernel,
        [kept((quarter, width), BF16), shape((expert_count, SLOTS, width), BF16)],
        *((x, "vmem") for x in parts),
        *((x, "vmem") for x in norm_parts),
        (select, "vmem"),
    )
    arrived = swapped(outgoing, "sp")

    cut = down_w.shape[0] // 4
    down_far = turned(down_left[:cut], 1), turned(down_right[cut:], -1)

    last = (merge, second_norm_gain.reshape(1, width), second_norm_bias.reshape(1, width))
    near_weights = (gate_w, up_w, gate_left, up_left)
    unit = gate_w.shape[1]
    base, *last, near = kernel_call(
        shared_kernel,
        [
            kept((quarter, width), F32),
            *(kept(x.shape, F32) for x in last),
            kept((len(near_weights) // 2, width, 2 * unit), BF16),
        ],
        (normed, "vmem"),
        shared_gate_weight,
        shared_up_weight,
        shared_down_weight,
        (last[0], "vmem"),
        *last[1:],
        *((w, "hbm") for w in near_weights),
        scratch=(pltpu.SemaphoreType.DMA((len(near_weights),)),),
    )
    weights = (gate_right, up_right, gate_far, up_far, down_w, down_left, down_right)
    acc, hidden = kernel_call(
        expert_kernel,
        [kept((slot_count, width), F32), kept((slot_count, unit), BF16)],
        (arrived, "vmem"),
        (near, "vmem"),
        *((w, "hbm") for w in weights),
        scratch=(
            pltpu.VMEM((2, width, 2 * unit), BF16),
            pltpu.VMEM((3 * unit, width), BF16),
            pltpu.SemaphoreType.DMA((len(weights),)),
        ),
    )
    leaving = kernel_call(
        last_kernel, kept((expert_count, SLOTS, width), BF16), (acc, "vmem"), (hidden, "vmem"), *down_far
    )
    returned = swapped(leaving, "sp")
    return kernel_call(
        merge_kernel, shape((quarter, width), BF16), (returned, "vmem"), (base, "vmem"), *((x, "vmem") for x in last)
    )


def solution(mesh):
    in_specs = (
        P(("sp", "tp"), None),
        P("sp", None, "tp"),
        P("sp", None, "tp"),
        P(None, None, "tp"),
        P(None, "tp", None, None),
        P(None, "tp", None, None),
        P(None, "tp"),
        P("sp", None, "tp"),
        P(None, "tp", None),
        P(),
        P(),
        P("sp", None),
        P("sp", None),
        P("sp", None, "tp"),
        P("sp", None, "tp"),
        P("sp", "tp", None),
        P(),
        P(),
        P(),
        P(),
        P(),
    )

    return jax.shard_map(shards, mesh=mesh, in_specs=in_specs, out_specs=P(("sp", "tp"), None), check_vma=False)
```

profile of v0, /device:TPU:1, one launch (start us, length us, event | category | flops | bytes accessed | tf_op | source)
XLA Modules:
  0.0 125.5 jit_solution(10682698774324096298)
XLA Ops:
  0.0 0.7 slice.16
  0.7 4.5 %collective-permute-start = (bf16[16,128]{1,0:T(8,128)(2,1)S(1)}, bf16[16,128]{1,0:T(8,128)(2,1)S(1)}, u32[]{:S(2)}, u32[]{:S(2)}) collective-permute-start(bf16[16,128]{1,0:T(8,128)(2,1)S(1)} %bitcast.35), channel_id=1, source_target_pairs={{0,4},{4,8},{8,12},{12,16},{16,20},{20,24},{24,28},{28,32},{32,36}... | collective-permute-start | bytes 12296 | tf_op jit(solution)/shard_map/ppermute | solution.py:327
  5.2 0.7 collective-permute-done.border
  5.9 3.0 %shard_map.199 = (f32[128,512]{1,0:T(8,128)S(1)}, f32[128,512]{1,0:T(8,128)S(1)}, bf16[64,8,128]{2,1,0:T(8,128)(2,1)}) custom-call(bf16[512,128]{1,0:T(8,128)(2,1)} %bitcast.29, bf16[16,128]{1,0:T(8,128)(2,1)S(1)} %collective-permute-done.border, bf16[4,2,256]{2,1,0:T(2,128)(2,1)} %taps.1, bf16[2,4,64,64]{3,2,1,0:T(8,128)(2,1)} %small_maps.1, ...), custom_call_target="tpu_custom_call" | custom-call | tf_op jit(solution)/shard_map/pallas_call | solution.py:27
  8.9 13.5 %all-to-all-start = ((bf16[64,8,128]{2,1,0:T(8,128)(2,1)}), bf16[64,8,128]{2,1,0:T(8,128)(2,1)S(1)}, u32[]{:S(2)}, u32[]{:S(2)}) async-start(bf16[64,8,128]{2,1,0:T(8,128)(2,1)} %get-tuple-element.30), calls=%async_computation | async-start | bytes 262144 | tf_op jit(solution)/shard_map/all_to_all | solution.py:290
  22.4 0.1 pad_add_fusion.places
  22.5 2.4 %shard_map.200 = (bf16[128,32]{1,0:T(8,128)(2,1)S(1)}, f32[32,128]{1,0:T(8,128)S(1)}, f32[128,512]{1,0:T(8,128)S(1)}, f32[128,512]{1,0:T(8,128)S(1)}, bf16[32,20...) custom-call(s32[2]{0:T(128)S(1)} %pad_add_fusion.places, ...), custom_call_target="tpu_custom_call" | custom-call | tf_op jit(solution)/shard_map/pallas_call | solution.py:27
  24.9 8.6 %all-to-all-done.spans = bf16[64,8,128]{2,1,0:T(8,128)(2,1)S(1)} async-done(((bf16[64,8,128]{2,1,0:T(8,128)(2,1)}), bf16[64,8,128]{2,1,0:T(8,128)(2,1)S(1)}, u32[]{:S(2)}, u32[]{:S(2)}) %all-to-all-start) | async-done | bytes 131104 | tf_op jit(solution)/shard_map/all_to_all | solution.py:290
  33.5 0.7 shard_map.201
  34.2 1.4 %collective-permute-start.1 = (bf16[32,2048]{1,0:T(8,128)(2,1)S(1)}, bf16[32,2048]{1,0:T(8,128)(2,1)S(1)}, u32[]{:S(2)}, u32[]{:S(2)}) collective-permute-start(bf16[32,2048]{1,0:T(8,128)(2,1)S(1)} %get-tuple-element.38), channel_id=1, source_target_pairs={{0,1},{1,2},{2,3},{3,0},{4,5},{5,6},{6,7},{7,4},{8,9},{9,10},{10,1... | collective-permute-start | bytes 393224 | tf_op jit(solution)/shard_map/ppermute | solution.py:286
  35.6 1.5 %collective-permute-start.2 = (bf16[32,2048]{1,0:T(8,128)(2,1)S(1)}, bf16[32,2048]{1,0:T(8,128)(2,1)S(1)}, u32[]{:S(2)}, u32[]{:S(2)}) collective-permute-start(bf16[32,2048]{1,0:T(8,128)(2,1)S(1)} %get-tuple-element.39), channel_id=1, source_target_pairs={{0,3},{1,0},{2,1},{3,2},{4,7},{5,4},{6,5},{7,6},{8,11},{9,8},{10,9... | collective-permute-start | bytes 393224 | tf_op jit(solution)/shard_map/ppermute | solution.py:286
  37.1 1.6 %collective-permute-start.3 = (bf16[32,2048]{1,0:T(8,128)(2,1)S(1)}, bf16[32,2048]{1,0:T(8,128)(2,1)S(1)}, u32[]{:S(2)}, u32[]{:S(2)}) collective-permute-start(bf16[32,2048]{1,0:T(8,128)(2,1)S(1)} %get-tuple-element.40), channel_id=1, source_target_pairs={{0,2},{1,3},{2,0},{3,1},{4,6},{5,7},{6,4},{7,5},{8,10},{9,11},{10,... | collective-permute-start | bytes 393224 | tf_op jit(solution)/shard_map/ppermute | solution.py:286
  38.6 0.4 collective-permute-start.4
  39.0 2.3 %collective-permute-start.7 = (bf16[2048,128]{1,0:T(8,128)(2,1)}, bf16[2048,128]{1,0:T(8,128)(2,1)}, u32[]{:S(2)}, u32[]{:S(2)}) collective-permute-start(bf16[2048,128]{1,0:T(8,128)(2,1)} %bitcast.20.u0), channel_id=1, source_target_pairs={{0,3},{1,0},{2,1},{3,2},{4,7},{5,4},{6,5},{7,6},{8,11},{9,8},{10,9... | collective-permute-start | bytes 1572872 | tf_op jit(solution)/shard_map/ppermute | solution.py:286
  41.3 0.0 collective-permute-done.1.refs_1_
  41.3 0.3 collective-permute-start.11
  41.7 0.0 collective-permute-done.2.refs_2_
  41.7 2.6 %collective-permute-done.3.refs_3_ = bf16[32,2048]{1,0:T(8,128)(2,1)S(1)} collective-permute-done((bf16[32,2048]{1,0:T(8,128)(2,1)S(1)}, bf16[32,2048]{1,0:T(8,128)(2,1)S(1)}, u32[]{:S(2)}, u32[]{:S(2)}) %collective-permute-start.3) | collective-permute-done | bytes 131104 | tf_op jit(solution)/shard_map/ppermute | solution.py:286
  44.2 1.4 %shard_map.202 = (bf16[32,2048]{1,0:T(8,128)(2,1)S(1)}, bf16[64,2,2048]{2,1,0:T(2,128)(2,1)}) custom-call(bf16[32,2048]{1,0:T(8,128)(2,1)S(1)} %get-tuple-element.37.refs_0_, bf16[32,2048]{1,0:T(8,128)(2,1)S(1)} %collective-permute-done.1.refs_1_, bf16[32,2048]{1,0:T(8,128)(2,1)S(1)} %collective-permute-done.2.refs_2_, ...), custom_call_target="tpu_custom_call" | custom-call | tf_op jit(solution)/shard_map/pallas_call | solution.py:27
  45.6 6.2 %all-to-all-start.1 = ((bf16[64,2,2048]{2,1,0:T(2,128)(2,1)}), bf16[64,2,2048]{2,1,0:T(2,128)(2,1)S(1)}, u32[]{:S(2)}, u32[]{:S(2)}) async-start(bf16[64,2,2048]{2,1,0:T(2,128)(2,1)} %get-tuple-element.45), calls=%async_computation.1 | async-start | bytes 1048576 | tf_op jit(solution)/shard_map/all_to_all | solution.py:290
  51.8 1.2 collective-permute-start.10
  52.9 0.1 collective-permute-start.5
  53.0 2.9 %collective-permute-done.4.g1 = bf16[2048,128]{1,0:T(8,128)(2,1)} collective-permute-done((bf16[2048,128]{1,0:T(8,128)(2,1)}, bf16[2048,128]{1,0:T(8,128)(2,1)}, u32[]{:S(2)}, u32[]{:S(2)}) %collective-permute-start.4) | collective-permute-done | bytes 524320 | tf_op jit(solution)/shard_map/ppermute | solution.py:286
  55.9 0.0 collective-permute-start.6
  55.9 0.0 collective-permute-done.7.u2
  55.9 1.5 %collective-permute-start.8 = (bf16[2048,128]{1,0:T(8,128)(2,1)}, bf16[2048,128]{1,0:T(8,128)(2,1)S(1)}, u32[]{:S(2)}, u32[]{:S(2)}) collective-permute-start(bf16[2048,128]{1,0:T(8,128)(2,1)} %collective-permute-done.4.g1), channel_id=1, source_target_pairs={{0,1},{1,2},{2,3},{3,0},{4,5},{5,6},{6,7},{7,4},{8,9},{9,10},{10,1... | collective-permute-start | bytes 1572872 | tf_op jit(solution)/shard_map/ppermute | solution.py:286
  57.4 8.2 %collective-permute-done.11.d2 = bf16[128,2048]{1,0:T(8,128)(2,1)S(1)} collective-permute-done((bf16[128,2048]{1,0:T(8,128)(2,1)}, bf16[128,2048]{1,0:T(8,128)(2,1)S(1)}, u32[]{:S(2)}, u32[]{:S(2)}) %collective-permute-start.11) | collective-permute-done | bytes 524320 | tf_op jit(solution)/shard_map/ppermute | solution.py:286
  65.6 0.0 copy-start
  65.6 2.7 %collective-permute-start.9 = (bf16[2048,128]{1,0:T(8,128)(2,1)}, bf16[2048,128]{1,0:T(8,128)(2,1)}, u32[]{:S(2)}, u32[]{:S(2)}) collective-permute-start(bf16[2048,128]{1,0:T(8,128)(2,1)} %collective-permute-done.7.u2), channel_id=1, source_target_pairs={{0,3},{1,0},{2,1},{3,2},{4,7},{5,4},{6,5},{7,6},{8,11},{9,8},{10,9... | collective-permute-start | bytes 1572872 | tf_op jit(solution)/shard_map/ppermute | solution.py:286
  68.3 0.8 slice.18
  69.1 0.0 collective-permute-done.10.d1
  69.1 0.0 copy-start.1
  69.1 0.1 collective-permute-start.13
  69.1 0.8 slice.17
  69.9 7.8 %collective-permute-done.5.u1 = bf16[2048,128]{1,0:T(8,128)(2,1)S(1)} collective-permute-done((bf16[2048,128]{1,0:T(8,128)(2,1)}, bf16[2048,128]{1,0:T(8,128)(2,1)S(1)}, u32[]{:S(2)}, u32[]{:S(2)}) %collective-permute-start.5) | collective-permute-done | bytes 524320 | tf_op jit(solution)/shard_map/ppermute | solution.py:286
  77.7 0.0 copy-start.4
  77.7 0.0 collective-permute-start.12
  77.7 0.0 copy-done
  77.7 0.0 copy-done.1
  77.7 0.8 copy-done.4
  78.5 4.4 %shard_map.203 = (f32[32,2048]{1,0:T(8,128)S(1)}, f32[32,128]{1,0:T(8,128)S(1)}, f32[1,2048]{1,0:T(1,128)S(1)}, f32[1,2048]{1,0:T(1,128)S(1)}, bf16[2,2048,256]{2,1,0:T(8,128)(2,1)S(1)}) custom-call(bf16[32,2048]{1,0:T(8,128)(2,1)S(1)} %get-tuple-element.46.normed, bf16[2048,512]{1,0:T(8,128)(2,1)} %gate_w.1, bf16[2048,512]{1,0:T(8,128)(2,1)} %up_w.1, ...), custom_call_target="tpu_custom_call" | custom-call | tf_op jit(solution)/shard_map/pallas_call | solution.py:27
  83.0 0.0 collective-permute-done.6.g2
  83.0 0.0 copy-start.2
  83.0 6.0 %collective-permute-done.8.g3 = bf16[2048,128]{1,0:T(8,128)(2,1)S(1)} collective-permute-done((bf16[2048,128]{1,0:T(8,128)(2,1)}, bf16[2048,128]{1,0:T(8,128)(2,1)S(1)}, u32[]{:S(2)}, u32[]{:S(2)}) %collective-permute-start.8) | collective-permute-done | bytes 524320 | tf_op jit(solution)/shard_map/ppermute | solution.py:286
  88.9 0.0 copy-done.2
  88.9 0.0 copy-start.3
  88.9 0.8 copy-done.3
  89.8 0.0 collective-permute-done.9.u3
  89.8 0.0 all-to-all-done.1.rows
  89.8 2.9 %shard_map.204 = (f32[128,2048]{1,0:T(8,128)S(1)}, bf16[128,128]{1,0:T(8,128)(2,1)S(1)}) custom-call(bf16[64,2,2048]{2,1,0:T(2,128)(2,1)S(1)} %all-to-all-done.1.rows, bf16[2,2048,256]{2,1,0:T(8,128)(2,1)S(1)} %get-tuple-element.48.near, bf16[2048,128]{1,0:T(8,128)(2,1)} %copy-done.2, bf16[2048,128]{1,0:T(8,128)(2,1)} %collective-permute-done.7.u2, ...), custom_call_target="tpu_custom_call" | custom-call | tf_op jit(solution)/shard_map/pallas_call | solution.py:27
  92.6 0.0 collective-permute-done.12.d3a
  92.6 3.9 %collective-permute-done.13.d3b = bf16[96,2048]{1,0:T(8,128)(2,1)S(1)} collective-permute-done((bf16[96,2048]{1,0:T(8,128)(2,1)}, bf16[96,2048]{1,0:T(8,128)(2,1)S(1)}, u32[]{:S(2)}, u32[]{:S(2)}) %collective-permute-start.13) | collective-permute-done | bytes 393248 | tf_op jit(solution)/shard_map/ppermute | solution.py:286
  96.5 0.0 copy-start.5
  96.5 0.8 copy-done.5
  97.3 1.4 %shard_map.205 = bf16[64,2,2048]{2,1,0:T(2,128)(2,1)S(1)} custom-call(f32[128,2048]{1,0:T(8,128)S(1)} %get-tuple-element.49.acc, bf16[128,128]{1,0:T(8,128)(2,1)S(1)} %get-tuple-element.50.hidden, bf16[32,2048]{1,0:T(8,128)(2,1)} %collective-permute-done.12.d3a, bf16[96,2048]{1,0:T(8,128)(2,1)} %copy-done.5), custom_call_target="tpu_custom_call" | custom-call | tf_op jit(solution)/shard_map/pallas_call | solution.py:27
  98.6 25.6 %all_to_all.15.returned = bf16[64,2,2048]{2,1,0:T(2,128)(2,1)S(1)} all-to-all(bf16[64,2,2048]{2,1,0:T(2,128)(2,1)S(1)} %shard_map.205), channel_id=1, replica_groups=mesh['sp'=64,'tp'=4] {'sp'}, dimensions={0} | all-to-all | bytes 1048576 | tf_op jit(solution)/shard_map/all_to_all | solution.py:290
  124.3 1.2 shard_map.206
Async XLA Ops:
  0.7 5.2 %collective-permute-start = (bf16[16,128]{1,0:T(8,128)(2,1)S(1)}, bf16[16,128]{1,0:T(8,128)(2,1)S(1)}, u32[]{:S(2)}, u32[]{:S(2)}) collective-permute-start(bf16[16,128]{1,0:T(8,128)(2,1)S(1)} %bitcast.35), channel_id=1, source_target_pairs={{0,4},{4,8},{8,12},{12,16},{16,20},{20,24},{24,28},{28,32},{32,36}... | collective-permute-start | bytes 12296 | tf_op jit(solution)/shard_map/ppermute | solution.py:327
  8.9 24.6 %all-to-all-start = ((bf16[64,8,128]{2,1,0:T(8,128)(2,1)}), bf16[64,8,128]{2,1,0:T(8,128)(2,1)S(1)}, u32[]{:S(2)}, u32[]{:S(2)}) async-start(bf16[64,8,128]{2,1,0:T(8,128)(2,1)} %get-tuple-element.30), calls=%async_computation | async-start | bytes 262144 | tf_op jit(solution)/shard_map/all_to_all | solution.py:290
  34.2 7.1 %collective-permute-start.1 = (bf16[32,2048]{1,0:T(8,128)(2,1)S(1)}, bf16[32,2048]{1,0:T(8,128)(2,1)S(1)}, u32[]{:S(2)}, u32[]{:S(2)}) collective-permute-start(bf16[32,2048]{1,0:T(8,128)(2,1)S(1)} %get-tuple-element.38), channel_id=1, source_target_pairs={{0,1},{1,2},{2,3},{3,0},{4,5},{5,6},{6,7},{7,4},{8,9},{9,10},{10,1... | collective-permute-start | bytes 393224 | tf_op jit(solution)/shard_map/ppermute | solution.py:286
  35.6 6.1 %collective-permute-start.2 = (bf16[32,2048]{1,0:T(8,128)(2,1)S(1)}, bf16[32,2048]{1,0:T(8,128)(2,1)S(1)}, u32[]{:S(2)}, u32[]{:S(2)}) collective-permute-start(bf16[32,2048]{1,0:T(8,128)(2,1)S(1)} %get-tuple-element.39), channel_id=1, source_target_pairs={{0,3},{1,0},{2,1},{3,2},{4,7},{5,4},{6,5},{7,6},{8,11},{9,8},{10,9... | collective-permute-start | bytes 393224 | tf_op jit(solution)/shard_map/ppermute | solution.py:286
  37.1 7.1 %collective-permute-start.3 = (bf16[32,2048]{1,0:T(8,128)(2,1)S(1)}, bf16[32,2048]{1,0:T(8,128)(2,1)S(1)}, u32[]{:S(2)}, u32[]{:S(2)}) collective-permute-start(bf16[32,2048]{1,0:T(8,128)(2,1)S(1)} %get-tuple-element.40), channel_id=1, source_target_pairs={{0,2},{1,3},{2,0},{3,1},{4,6},{5,7},{6,4},{7,5},{8,10},{9,11},{10,... | collective-permute-start | bytes 393224 | tf_op jit(solution)/shard_map/ppermute | solution.py:286
  38.6 17.3 %collective-permute-start.4 = (bf16[2048,128]{1,0:T(8,128)(2,1)}, bf16[2048,128]{1,0:T(8,128)(2,1)}, u32[]{:S(2)}, u32[]{:S(2)}) collective-permute-start(bf16[2048,128]{1,0:T(8,128)(2,1)} %bitcast.19.g0), channel_id=1, source_target_pairs={{0,1},{1,2},{2,3},{3,0},{4,5},{5,6},{6,7},{7,4},{8,9},{9,10},{10,1... | collective-permute-start | bytes 1572872 | tf_op jit(solution)/shard_map/ppermute | solution.py:286
  39.0 16.9 %collective-permute-start.7 = (bf16[2048,128]{1,0:T(8,128)(2,1)}, bf16[2048,128]{1,0:T(8,128)(2,1)}, u32[]{:S(2)}, u32[]{:S(2)}) collective-permute-start(bf16[2048,128]{1,0:T(8,128)(2,1)} %bitcast.20.u0), channel_id=1, source_target_pairs={{0,3},{1,0},{2,1},{3,2},{4,7},{5,4},{6,5},{7,6},{8,11},{9,8},{10,9... | collective-permute-start | bytes 1572872 | tf_op jit(solution)/shard_map/ppermute | solution.py:286
  41.3 24.3 %collective-permute-start.11 = (bf16[128,2048]{1,0:T(8,128)(2,1)}, bf16[128,2048]{1,0:T(8,128)(2,1)S(1)}, u32[]{:S(2)}, u32[]{:S(2)}) collective-permute-start(bf16[128,2048]{1,0:T(8,128)(2,1)} %bitcast.21.d0), channel_id=1, source_target_pairs={{0,3},{1,0},{2,1},{3,2},{4,7},{5,4},{6,5},{7,6},{8,11},{9,8},{10,9... | collective-permute-start | bytes 1572872 | tf_op jit(solution)/shard_map/ppermute | solution.py:286
  45.6 44.2 %all-to-all-start.1 = ((bf16[64,2,2048]{2,1,0:T(2,128)(2,1)}), bf16[64,2,2048]{2,1,0:T(2,128)(2,1)S(1)}, u32[]{:S(2)}, u32[]{:S(2)}) async-start(bf16[64,2,2048]{2,1,0:T(2,128)(2,1)} %get-tuple-element.45), calls=%async_computation.1 | async-start | bytes 1048576 | tf_op jit(solution)/shard_map/all_to_all | solution.py:290
  51.8 17.3 %collective-permute-start.10 = (bf16[128,2048]{1,0:T(8,128)(2,1)}, bf16[128,2048]{1,0:T(8,128)(2,1)S(1)}, u32[]{:S(2)}, u32[]{:S(2)}) collective-permute-start(bf16[128,2048]{1,0:T(8,128)(2,1)} %bitcast.21.d0), channel_id=1, source_target_pairs={{0,1},{1,2},{2,3},{3,0},{4,5},{5,6},{6,7},{7,4},{8,9},{9,10},{10,1... | collective-permute-start | bytes 1572872 | tf_op jit(solution)/shard_map/ppermute | solution.py:286
  52.9 24.8 %collective-permute-start.5 = (bf16[2048,128]{1,0:T(8,128)(2,1)}, bf16[2048,128]{1,0:T(8,128)(2,1)S(1)}, u32[]{:S(2)}, u32[]{:S(2)}) collective-permute-start(bf16[2048,128]{1,0:T(8,128)(2,1)} %bitcast.20.u0), channel_id=1, source_target_pairs={{0,1},{1,2},{2,3},{3,0},{4,5},{5,6},{6,7},{7,4},{8,9},{9,10},{10,1... | collective-permute-start | bytes 1572872 | tf_op jit(solution)/shard_map/ppermute | solution.py:286
  55.9 27.1 %collective-permute-start.6 = (bf16[2048,128]{1,0:T(8,128)(2,1)}, bf16[2048,128]{1,0:T(8,128)(2,1)S(1)}, u32[]{:S(2)}, u32[]{:S(2)}) collective-permute-start(bf16[2048,128]{1,0:T(8,128)(2,1)} %bitcast.19.g0), channel_id=1, source_target_pairs={{0,3},{1,0},{2,1},{3,2},{4,7},{5,4},{6,5},{7,6},{8,11},{9,8},{10,9... | collective-permute-start | bytes 1572872 | tf_op jit(solution)/shard_map/ppermute | solution.py:286
  55.9 33.0 %collective-permute-start.8 = (bf16[2048,128]{1,0:T(8,128)(2,1)}, bf16[2048,128]{1,0:T(8,128)(2,1)S(1)}, u32[]{:S(2)}, u32[]{:S(2)}) collective-permute-start(bf16[2048,128]{1,0:T(8,128)(2,1)} %collective-permute-done.4.g1), channel_id=1, source_target_pairs={{0,1},{1,2},{2,3},{3,0},{4,5},{5,6},{6,7},{7,4},{8,9},{9,10},{10,1... | collective-permute-start | bytes 1572872 | tf_op jit(solution)/shard_map/ppermute | solution.py:286
  65.6 12.1 %copy-start = (bf16[128,2048]{1,0:T(8,128)(2,1)}, bf16[128,2048]{1,0:T(8,128)(2,1)S(1)}, u32[]{:S(2)}) copy-start(bf16[128,2048]{1,0:T(8,128)(2,1)S(1)} %collective-permute-done.11.d2) | copy-start | bytes 1572868
  65.6 24.1 %collective-permute-start.9 = (bf16[2048,128]{1,0:T(8,128)(2,1)}, bf16[2048,128]{1,0:T(8,128)(2,1)}, u32[]{:S(2)}, u32[]{:S(2)}) collective-permute-start(bf16[2048,128]{1,0:T(8,128)(2,1)} %collective-permute-done.7.u2), channel_id=1, source_target_pairs={{0,3},{1,0},{2,1},{3,2},{4,7},{5,4},{6,5},{7,6},{8,11},{9,8},{10,9... | collective-permute-start | bytes 1572872 | tf_op jit(solution)/shard_map/ppermute | solution.py:286
  69.1 8.6 %copy-start.1 = (bf16[128,2048]{1,0:T(8,128)(2,1)}, bf16[128,2048]{1,0:T(8,128)(2,1)S(1)}, u32[]{:S(2)}) copy-start(bf16[128,2048]{1,0:T(8,128)(2,1)S(1)} %collective-permute-done.10.d1) | copy-start | bytes 1572868
  69.1 27.4 %collective-permute-start.13 = (bf16[96,2048]{1,0:T(8,128)(2,1)}, bf16[96,2048]{1,0:T(8,128)(2,1)S(1)}, u32[]{:S(2)}, u32[]{:S(2)}) collective-permute-start(bf16[96,2048]{1,0:T(8,128)(2,1)} %slice.18), channel_id=1, source_target_pairs={{0,3},{1,0},{2,1},{3,2},{4,7},{5,4},{6,5},{7,6},{8,11},{9,8},{10,9... | collective-permute-start | bytes 1179656 | tf_op jit(solution)/shard_map/ppermute | solution.py:286
  77.7 0.8 copy-start.4
  77.7 14.9 %collective-permute-start.12 = (bf16[32,2048]{1,0:T(8,128)(2,1)}, bf16[32,2048]{1,0:T(8,128)(2,1)}, u32[]{:S(2)}, u32[]{:S(2)}) collective-permute-start(bf16[32,2048]{1,0:T(8,128)(2,1)} %slice.17), channel_id=1, source_target_pairs={{0,1},{1,2},{2,3},{3,0},{4,5},{5,6},{6,7},{7,4},{8,9},{9,10},{10,1... | collective-permute-start | bytes 393224 | tf_op jit(solution)/shard_map/ppermute | solution.py:286
  83.0 6.0 %copy-start.2 = (bf16[2048,128]{1,0:T(8,128)(2,1)}, bf16[2048,128]{1,0:T(8,128)(2,1)S(1)}, u32[]{:S(2)}) copy-start(bf16[2048,128]{1,0:T(8,128)(2,1)S(1)} %collective-permute-done.6.g2) | copy-start | bytes 1572868
  88.9 0.8 copy-start.3
  96.5 0.8 copy-start.5
where the time goes:
time: 126 us; the launch traced here: 125 us
  waiting for transfers between devices  40.7 us (32%)
  starting transfers between devices  37.1 us (29%)
  blocking collectives  25.6 us (20%)
  Pallas kernels  17.3 us (14%)
  local copies, waits for them, and re-layouts  4.57 us (4%)
    ppermute x13, waiting for transfers between devices, turned(): lax.ppermute(shard, 'tp', [(i, (i + by) % count) for i in range(count)])  31.4 us
    all_to_all x1, blocking collectives, swapped(): return lax.all_to_all(pieces, axis, 0, 0, tiled=True)  25.6 us
    all_to_all x2, starting transfers between devices, swapped(): return lax.all_to_all(pieces, axis, 0, 0, tiled=True)  19.7 us
    pallas_call x8, Pallas kernels, kernel_call(): pl.pallas_call(body, out_shape=out_shape, in_specs=specs, out_specs=[VMEM...  17.3 us
    ppermute x13, starting transfers between devices, turned(): lax.ppermute(shard, 'tp', [(i, (i + by) % count) for i in range(count)])  12.9 us
    all_to_all x2, waiting for transfers between devices, swapped(): return lax.all_to_all(pieces, axis, 0, 0, tiled=True)  8.6 us
    ppermute x1, starting transfers between devices, shards(): lax.ppermute(rows[rows.shape[0] - margin:], 'sp', [(i, i + 1) for i in ra...  4.49 us
  transfers between devices with their start and end apart: 16, of which 8 were waited for; matrix products, arithmetic and copies ran while one was open for 1% of the time, Pallas kernels for 9%

commit v1 on v0

--- a/solution.py
+++ b/solution.py
@@ -90,7 +90,17 @@
     return array.reshape(length, groups, half // LANES, LANES).transpose(0, 2, 1, 3).reshape(-1, LANES)
 
 
-def local_kernel(rows, border, taps, small_maps, large_maps, decay_param, extra, decays, states, totals, padded, maps):
+def load_kernel(*refs):
+    count = (len(refs) - 2) // 2
+    far, near, edge, sems = refs[:count], refs[count : 2 * count], refs[-2], refs[-1]
+    copies = fetched(list(zip(far, near)), sems)
+    copies[0].wait()
+    edge[...] = near[0][near[0].shape[0] - edge.shape[0] :]
+    for copy in copies[1:]:
+        copy.wait()
+
+
+def local_kernel(rows, taps, small_maps, large_maps, decay_param, extra, border, decays, states, totals, padded, maps):
     groups, half = decay_param.shape
     per_half = half // LANES
     step = groups * per_half
@@ -101,9 +111,16 @@
     margin = border.shape[0]
     padded[0:margin] = border[...].astype(F32)
     padded[margin:] = rows[...].astype(F32)
+    head = small_maps.shape[-1]
+    per_run = LANES // head
+    maps[...] = jnp.zeros(maps.shape, BF16)
+    for c in range(per_half):
+        for m in range(2):
+            for h in range(per_run):
+                at = h * head
+                maps[c, at : at + head, m * LANES + at : m * LANES + at + head] = small_maps[m, c * per_run + h]
     logs, ends = [], []
-    for g, blocks in enumerate((small_maps, large_maps)):
-        conv_runs = []
+    for g in range(groups):
         for c in range(per_half):
             at = slice(c * LANES, (c + 1) * LANES)
             summed = None
@@ -111,19 +128,11 @@
                 start = margin - (tap_count - 1 - k) * step + c * groups + g
                 term = tap_weights[k, g : g + 1, at] * padded[pl.ds(start, length, stride=step), :]
                 summed = term if summed is None else summed + term
-            conv_runs.append(summed.astype(BF16))
-        conv_rows = jnp.concatenate(conv_runs, axis=1)
-        maps[...] = jnp.zeros(maps.shape, BF16)
-        head = blocks.shape[-1]
-        for m in range(2):
-            for h in range(blocks.shape[1]):
-                maps[h * head : (h + 1) * head, m * half + h * head : m * half + (h + 1) * head] = blocks[m, h]
-        gates = jax.nn.sigmoid(dot(conv_rows, maps[...]))
-        for c in range(per_half):
-            at = slice(c * LANES, (c + 1) * LANES)
-            log_decay = gates[:, at] * rate[g : g + 1, at] + extra[pl.ds(c * groups + g, length, stride=step), :]
-            gate = gates[:, half + c * LANES : half + (c + 1) * LANES]
-            drive = jnp.sqrt(-expm1(2.0 * log_decay)) * gate * conv_runs[c].astype(F32)
+            conv_rows = summed.astype(BF16)
+            both = maps[c] if g == 0 else jnp.concatenate([large_maps[0, c], large_maps[1, c]], axis=1)
+            gates = jax.nn.sigmoid(dot(conv_rows, both))
+            log_decay = gates[:, :LANES] * rate[g : g + 1, at] + extra[pl.ds(c * groups + g, length, stride=step), :]
+            drive = jnp.sqrt(-expm1(2.0 * log_decay)) * gates[:, LANES:] * conv_rows.astype(F32)
             product, state = chain_rows(jnp.exp(log_decay), drive)
             to = slice((g * per_half + c) * LANES, (g * per_half + c + 1) * LANES)
             decays[:, to] = product
@@ -324,25 +333,36 @@
 
     rows = flat(recurrence_input)
     margin = 16
-    border = lax.ppermute(rows[rows.shape[0] - margin :], "sp", [(i, i + 1) for i in range(sp_count - 1)])
-
-    gate_w, up_w, down_w = routed_gate_weight[0], routed_up_weight[0], routed_down_weight[0]
-    gate_left, up_right = turned(gate_w, 1), turned(up_w, -1)
-    up_left, gate_right = turned(up_w, 1), turned(gate_w, -1)
-    down_left, down_right = turned(down_w, 1), turned(down_w, -1)
-
-    runs = channels // LANES
-    decays, states, totals = kernel_call(
-        local_kernel,
-        [kept((length, channels), F32), kept((length, channels), F32), shape((sp_count, 2 * runs, LANES), BF16)],
+    operands = (
         rows,
-        (border, "vmem"),
         convolution_taps,
         first_group_gates,
         second_group_gates,
         channel_decay,
         flat(position_log_extra),
-        scratch=(pltpu.VMEM((margin + rows.shape[0], LANES), F32), pltpu.VMEM((half, 2 * half), BF16)),
+    )
+    *operands, edge = kernel_call(
+        load_kernel,
+        [*(kept(x.shape, x.dtype) for x in operands), kept((margin, LANES), BF16)],
+        *((x, "hbm") for x in operands),
+        scratch=(pltpu.SemaphoreType.DMA((len(operands),)),),
+    )
+    border = lax.ppermute(edge, "sp", [(i, i + 1) for i in range(sp_count - 1)])
+
+    gate_w, up_w, down_w = routed_gate_weight[0], routed_up_weight[0], routed_down_weight[0]
+    gate_left, up_right = turned(gate_w, 1), turned(up_w, -1)
+    up_left, gate_right = turned(up_w, 1), turned(gate_w, -1)
+    down_left, down_right = turned(down_w, 1), turned(down_w, -1)
+
+    runs = channels // LANES
+    decays, states, totals = kernel_call(
+        local_kernel,
+        [kept((length, channels), F32), kept((length, channels), F32), shape((sp_count, 2 * runs, LANES), BF16)],
+        *((x, "vmem") for x in (*operands, border)),
+        scratch=(
+            pltpu.VMEM((margin + rows.shape[0], LANES), F32),
+            pltpu.VMEM((half // LANES, LANES, 2 * LANES), BF16),
+        ),
     )
     spans = swapped(totals, "sp")
 
@@ -401,7 +421,7 @@
     )
     arrived = swapped(outgoing, "sp")
 
-    cut = down_w.shape[0] // 4
+    cut = down_w.shape[0] // 2
     down_far = turned(down_left[:cut], 1), turned(down_right[cut:], -1)
 
     last = (merge, second_norm_gain.reshape(1, width), second_norm_bias.reshape(1, width))

time: 126 us -> 124 us (0.984)
  local copies, waits for them, and re-layouts: 4.57 us -> 2.32 us
  blocking collectives: 25.6 us -> 26.9 us
    all_to_all x1, blocking collectives: 25.6 us -> 26.9 us  [swapped(): return lax.all_to_all(pieces, axis, 0, 0, tiled=True)]
    pallas_call x8 -> x9, Pallas kernels: 17.3 us -> 17.2 us  [kernel_call(): pl.pallas_call(body, out_shape=out_shape, in_specs=specs, out_specs=[VMEM...]
where the time goes in v1:
time: 124 us
  waiting for transfers between devices  41.4 us (33%)
  starting transfers between devices  35.9 us (29%)
  blocking collectives  26.9 us (22%)
  Pallas kernels  17.2 us (14%)
  local copies, waits for them, and re-layouts  2.32 us (2%)
    ppermute x13, waiting for transfers between devices, turned(): lax.ppermute(shard, 'tp', [(i, (i + by) % count) for i in range(count)])  32.1 us
    all_to_all x1, blocking collectives, swapped(): return lax.all_to_all(pieces, axis, 0, 0, tiled=True)  26.9 us
    all_to_all x2, starting transfers between devices, swapped(): return lax.all_to_all(pieces, axis, 0, 0, tiled=True)  19.7 us
    pallas_call x9, Pallas kernels, kernel_call(): pl.pallas_call(body, out_shape=out_shape, in_specs=specs, out_specs=[VMEM...  17.2 us
    ppermute x13, starting transfers between devices, turned(): lax.ppermute(shard, 'tp', [(i, (i + by) % count) for i in range(count)])  11.7 us
    all_to_all x2, waiting for transfers between devices, swapped(): return lax.all_to_all(pieces, axis, 0, 0, tiled=True)  8.6 us
    ppermute x1, starting transfers between devices, shards(): border = lax.ppermute(edge, 'sp', [(i, i + 1) for i in range(sp_count - 1)])  4.5 us
  transfers between devices with their start and end apart: 16, of which 8 were waited for; matrix products, arithmetic and copies ran while one was open for 1% of the time, Pallas kernels for 9%

profile of v1, /device:TPU:1, one launch (start us, length us, event | category | flops | bytes accessed | tf_op | source)
XLA Modules:
  0.0 124.0 jit_solution(10568265403871366280)
XLA Ops:
  0.0 1.2 shard_map.199
  1.2 4.5 %collective-permute-start = (bf16[16,128]{1,0:T(8,128)(2,1)S(1)}, bf16[16,128]{1,0:T(8,128)(2,1)S(1)}, u32[]{:S(2)}, u32[]{:S(2)}) collective-permute-start(bf16[16,128]{1,0:T(8,128)(2,1)S(1)} %get-tuple-element.43), channel_id=1, source_target_pairs={{0,4},{4,8},{8,12},{12,16},{16,20},{20,24},{24,28},{28,32},{32,36}... | collective-permute-start | bytes 12296 | tf_op jit(solution)/shard_map/ppermute | solution.py:350
  5.7 0.7 collective-permute-done.border
  6.5 1.7 %shard_map.200 = (f32[128,512]{1,0:T(8,128)S(1)}, f32[128,512]{1,0:T(8,128)S(1)}, bf16[64,8,128]{2,1,0:T(8,128)(2,1)}) custom-call(bf16[512,128]{1,0:T(8,128)(2,1)S(1)} %get-tuple-element.37.rows, bf16[4,2,256]{2,1,0:T(2,128)(2,1)S(1)} %get-tuple-element.38.taps, bf16[2,4,64,64]{3,2,1,0:T(8,128)(2,1)S(1)} %get-tuple-element.39.small_maps, ...), custom_call_target="tpu_custom_call" | custom-call | tf_op jit(solution)/shard_map/pallas_call | solution.py:27
  8.2 13.5 %all-to-all-start = ((bf16[64,8,128]{2,1,0:T(8,128)(2,1)}), bf16[64,8,128]{2,1,0:T(8,128)(2,1)S(1)}, u32[]{:S(2)}, u32[]{:S(2)}) async-start(bf16[64,8,128]{2,1,0:T(8,128)(2,1)} %get-tuple-element.44), calls=%async_computation | async-start | bytes 262144 | tf_op jit(solution)/shard_map/all_to_all | solution.py:299
  21.8 0.1 pad_add_fusion.places
  21.8 2.4 %shard_map.201 = (bf16[128,32]{1,0:T(8,128)(2,1)S(1)}, f32[32,128]{1,0:T(8,128)S(1)}, f32[128,512]{1,0:T(8,128)S(1)}, f32[128,512]{1,0:T(8,128)S(1)}, bf16[32,20...) custom-call(s32[2]{0:T(128)S(1)} %pad_add_fusion.places, ...), custom_call_target="tpu_custom_call" | custom-call | tf_op jit(solution)/shard_map/pallas_call | solution.py:27
  24.2 8.6 %all-to-all-done.spans = bf16[64,8,128]{2,1,0:T(8,128)(2,1)S(1)} async-done(((bf16[64,8,128]{2,1,0:T(8,128)(2,1)}), bf16[64,8,128]{2,1,0:T(8,128)(2,1)S(1)}, u32[]{:S(2)}, u32[]{:S(2)}) %all-to-all-start) | async-done | bytes 131104 | tf_op jit(solution)/shard_map/all_to_all | solution.py:299
  32.8 0.7 shard_map.202
  33.5 1.4 %collective-permute-start.1 = (bf16[32,2048]{1,0:T(8,128)(2,1)S(1)}, bf16[32,2048]{1,0:T(8,128)(2,1)S(1)}, u32[]{:S(2)}, u32[]{:S(2)}) collective-permute-start(bf16[32,2048]{1,0:T(8,128)(2,1)S(1)} %get-tuple-element.52), channel_id=1, source_target_pairs={{0,1},{1,2},{2,3},{3,0},{4,5},{5,6},{6,7},{7,4},{8,9},{9,10},{10,1... | collective-permute-start | bytes 393224 | tf_op jit(solution)/shard_map/ppermute | solution.py:295
  34.9 1.5 %collective-permute-start.2 = (bf16[32,2048]{1,0:T(8,128)(2,1)S(1)}, bf16[32,2048]{1,0:T(8,128)(2,1)S(1)}, u32[]{:S(2)}, u32[]{:S(2)}) collective-permute-start(bf16[32,2048]{1,0:T(8,128)(2,1)S(1)} %get-tuple-element.53), channel_id=1, source_target_pairs={{0,3},{1,0},{2,1},{3,2},{4,7},{5,4},{6,5},{7,6},{8,11},{9,8},{10,9... | collective-permute-start | bytes 393224 | tf_op jit(solution)/shard_map/ppermute | solution.py:295
  36.4 1.6 %collective-permute-start.3 = (bf16[32,2048]{1,0:T(8,128)(2,1)S(1)}, bf16[32,2048]{1,0:T(8,128)(2,1)S(1)}, u32[]{:S(2)}, u32[]{:S(2)}) collective-permute-start(bf16[32,2048]{1,0:T(8,128)(2,1)S(1)} %get-tuple-element.54), channel_id=1, source_target_pairs={{0,2},{1,3},{2,0},{3,1},{4,6},{5,7},{6,4},{7,5},{8,10},{9,11},{10,... | collective-permute-start | bytes 393224 | tf_op jit(solution)/shard_map/ppermute | solution.py:295
  38.0 0.4 collective-permute-start.4
  38.4 2.3 %collective-permute-start.7 = (bf16[2048,128]{1,0:T(8,128)(2,1)}, bf16[2048,128]{1,0:T(8,128)(2,1)}, u32[]{:S(2)}, u32[]{:S(2)}) collective-permute-start(bf16[2048,128]{1,0:T(8,128)(2,1)} %bitcast.18.u0), channel_id=1, source_target_pairs={{0,3},{1,0},{2,1},{3,2},{4,7},{5,4},{6,5},{7,6},{8,11},{9,8},{10,9... | collective-permute-start | bytes 1572872 | tf_op jit(solution)/shard_map/ppermute | solution.py:295
  40.6 0.0 collective-permute-done.1.refs_1_
  40.6 0.0 collective-permute-start.10
  40.6 0.0 collective-permute-done.2.refs_2_
  40.7 2.9 %collective-permute-done.3.refs_3_ = bf16[32,2048]{1,0:T(8,128)(2,1)S(1)} collective-permute-done((bf16[32,2048]{1,0:T(8,128)(2,1)S(1)}, bf16[32,2048]{1,0:T(8,128)(2,1)S(1)}, u32[]{:S(2)}, u32[]{:S(2)}) %collective-permute-start.3) | collective-permute-done | bytes 131104 | tf_op jit(solution)/shard_map/ppermute | solution.py:295
  43.5 1.4 %shard_map.203 = (bf16[32,2048]{1,0:T(8,128)(2,1)S(1)}, bf16[64,2,2048]{2,1,0:T(2,128)(2,1)}) custom-call(bf16[32,2048]{1,0:T(8,128)(2,1)S(1)} %get-tuple-element.51.refs_0_, bf16[32,2048]{1,0:T(8,128)(2,1)S(1)} %collective-permute-done.1.refs_1_, bf16[32,2048]{1,0:T(8,128)(2,1)S(1)} %collective-permute-done.2.refs_2_, ...), custom_call_target="tpu_custom_call" | custom-call | tf_op jit(solution)/shard_map/pallas_call | solution.py:27
  44.9 6.2 %all-to-all-start.1 = ((bf16[64,2,2048]{2,1,0:T(2,128)(2,1)}), bf16[64,2,2048]{2,1,0:T(2,128)(2,1)S(1)}, u32[]{:S(2)}, u32[]{:S(2)}) async-start(bf16[64,2,2048]{2,1,0:T(2,128)(2,1)} %get-tuple-element.59), calls=%async_computation.1 | async-start | bytes 1048576 | tf_op jit(solution)/shard_map/all_to_all | solution.py:299
  51.1 1.3 %collective-permute-start.11 = (bf16[128,2048]{1,0:T(8,128)(2,1)}, bf16[128,2048]{1,0:T(8,128)(2,1)S(1)}, u32[]{:S(2)}, u32[]{:S(2)}) collective-permute-start(bf16[128,2048]{1,0:T(8,128)(2,1)} %bitcast.19.d0), channel_id=1, source_target_pairs={{0,3},{1,0},{2,1},{3,2},{4,7},{5,4},{6,5},{7,6},{8,11},{9,8},{10,9... | collective-permute-start | bytes 1572872 | tf_op jit(solution)/shard_map/ppermute | solution.py:295
  52.4 0.3 collective-permute-start.5
  52.7 2.6 %collective-permute-done.4.g1 = bf16[2048,128]{1,0:T(8,128)(2,1)} collective-permute-done((bf16[2048,128]{1,0:T(8,128)(2,1)}, bf16[2048,128]{1,0:T(8,128)(2,1)}, u32[]{:S(2)}, u32[]{:S(2)}) %collective-permute-start.4) | collective-permute-done | bytes 524320 | tf_op jit(solution)/shard_map/ppermute | solution.py:295
  55.2 0.0 collective-permute-start.6
  55.2 0.0 collective-permute-done.7.u2
  55.2 1.5 %collective-permute-start.8 = (bf16[2048,128]{1,0:T(8,128)(2,1)}, bf16[2048,128]{1,0:T(8,128)(2,1)S(1)}, u32[]{:S(2)}, u32[]{:S(2)}) collective-permute-start(bf16[2048,128]{1,0:T(8,128)(2,1)} %collective-permute-done.4.g1), channel_id=1, source_target_pairs={{0,1},{1,2},{2,3},{3,0},{4,5},{5,6},{6,7},{7,4},{8,9},{9,10},{10,1... | collective-permute-start | bytes 1572872 | tf_op jit(solution)/shard_map/ppermute | solution.py:295
  56.7 9.7 %collective-permute-done.10.d1 = bf16[128,2048]{1,0:T(8,128)(2,1)S(1)} collective-permute-done((bf16[128,2048]{1,0:T(8,128)(2,1)}, bf16[128,2048]{1,0:T(8,128)(2,1)S(1)}, u32[]{:S(2)}, u32[]{:S(2)}) %collective-permute-start.10) | collective-permute-done | bytes 524320 | tf_op jit(solution)/shard_map/ppermute | solution.py:295
  66.3 0.0 copy-start
  66.3 0.0 collective-permute-start.9
  66.4 0.0 collective-permute-done.11.d2
  66.4 0.0 copy-start.1
  66.4 1.5 %collective-permute-start.12 = (bf16[64,2048]{1,0:T(8,128)(2,1)S(1)}, bf16[64,2048]{1,0:T(8,128)(2,1)}, u32[]{:S(2)}, u32[]{:S(2)}) collective-permute-start(bf16[64,2048]{1,0:T(8,128)(2,1)S(1)} %slice.8), channel_id=1, source_target_pairs={{0,1},{1,2},{2,3},{3,0},{4,5},{5,6},{6,7},{7,4},{8,9},{9,10},{10,1... | collective-permute-start | bytes 786440 | tf_op jit(solution)/shard_map/ppermute | solution.py:295
  67.9 0.7 slice.9
  68.6 8.9 %collective-permute-done.5.u1 = bf16[2048,128]{1,0:T(8,128)(2,1)S(1)} collective-permute-done((bf16[2048,128]{1,0:T(8,128)(2,1)}, bf16[2048,128]{1,0:T(8,128)(2,1)S(1)}, u32[]{:S(2)}, u32[]{:S(2)}) %collective-permute-start.5) | collective-permute-done | bytes 524320 | tf_op jit(solution)/shard_map/ppermute | solution.py:295
  77.6 0.0 copy-start.4
  77.6 0.0 collective-permute-start.13
  77.6 0.0 copy-done
  77.6 0.0 copy-done.1
  77.6 0.8 copy-done.4
  78.4 4.4 %shard_map.204 = (f32[32,2048]{1,0:T(8,128)S(1)}, f32[32,128]{1,0:T(8,128)S(1)}, f32[1,2048]{1,0:T(1,128)S(1)}, f32[1,2048]{1,0:T(1,128)S(1)}, bf16[2,2048,256]{2,1,0:T(8,128)(2,1)S(1)}) custom-call(bf16[32,2048]{1,0:T(8,128)(2,1)S(1)} %get-tuple-element.60.normed, bf16[2048,512]{1,0:T(8,128)(2,1)} %gate_w.1, bf16[2048,512]{1,0:T(8,128)(2,1)} %up_w.1, ...), custom_call_target="tpu_custom_call" | custom-call | tf_op jit(solution)/shard_map/pallas_call | solution.py:27
  82.8 0.0 collective-permute-done.6.g2
  82.8 0.0 copy-start.2
  82.8 6.0 %collective-permute-done.8.g3 = bf16[2048,128]{1,0:T(8,128)(2,1)S(1)} collective-permute-done((bf16[2048,128]{1,0:T(8,128)(2,1)}, bf16[2048,128]{1,0:T(8,128)(2,1)S(1)}, u32[]{:S(2)}, u32[]{:S(2)}) %collective-permute-start.8) | collective-permute-done | bytes 524320 | tf_op jit(solution)/shard_map/ppermute | solution.py:295
  88.8 0.0 copy-done.2
  88.8 0.0 copy-start.3
  88.8 0.8 copy-done.3
  89.6 0.0 collective-permute-done.9.u3
  89.6 0.0 all-to-all-done.1.rows
  89.6 2.9 %shard_map.205 = (f32[128,2048]{1,0:T(8,128)S(1)}, bf16[128,128]{1,0:T(8,128)(2,1)S(1)}) custom-call(bf16[64,2,2048]{2,1,0:T(2,128)(2,1)S(1)} %all-to-all-done.1.rows, bf16[2,2048,256]{2,1,0:T(8,128)(2,1)S(1)} %get-tuple-element.62.near, bf16[2048,128]{1,0:T(8,128)(2,1)} %copy-done.2, bf16[2048,128]{1,0:T(8,128)(2,1)} %collective-permute-done.7.u2, ...), custom_call_target="tpu_custom_call" | custom-call | tf_op jit(solution)/shard_map/pallas_call | solution.py:27
  92.5 2.1 %collective-permute-done.12.d3a = bf16[64,2048]{1,0:T(8,128)(2,1)} collective-permute-done((bf16[64,2048]{1,0:T(8,128)(2,1)S(1)}, bf16[64,2048]{1,0:T(8,128)(2,1)}, u32[]{:S(2)}, u32[]{:S(2)}) %collective-permute-start.12) | collective-permute-done | bytes 262176 | tf_op jit(solution)/shard_map/ppermute | solution.py:295
  94.5 0.0 collective-permute-done.13.d3b
  94.5 1.3 %shard_map.206 = bf16[64,2,2048]{2,1,0:T(2,128)(2,1)S(1)} custom-call(f32[128,2048]{1,0:T(8,128)S(1)} %get-tuple-element.63.acc, bf16[128,128]{1,0:T(8,128)(2,1)S(1)} %get-tuple-element.64.hidden, bf16[64,2048]{1,0:T(8,128)(2,1)} %collective-permute-done.12.d3a, bf16[64,2048]{1,0:T(8,128)(2,1)} %collective-permute-done.13.d3b), custom_call_target="tpu_custom_call" | custom-call | tf_op jit(solution)/shard_map/pallas_call | solution.py:27
  95.9 26.9 %all_to_all.15.returned = bf16[64,2,2048]{2,1,0:T(2,128)(2,1)S(1)} all-to-all(bf16[64,2,2048]{2,1,0:T(2,128)(2,1)S(1)} %shard_map.206), channel_id=1, replica_groups=mesh['sp'=64,'tp'=4] {'sp'}, dimensions={0} | all-to-all | bytes 1048576 | tf_op jit(solution)/shard_map/all_to_all | solution.py:299
  122.8 1.2 shard_map.207
  (1 shorter events, 0.0 us)
Async XLA Ops:
  1.2 5.2 %collective-permute-start = (bf16[16,128]{1,0:T(8,128)(2,1)S(1)}, bf16[16,128]{1,0:T(8,128)(2,1)S(1)}, u32[]{:S(2)}, u32[]{:S(2)}) collective-permute-start(bf16[16,128]{1,0:T(8,128)(2,1)S(1)} %get-tuple-element.43), channel_id=1, source_target_pairs={{0,4},{4,8},{8,12},{12,16},{16,20},{20,24},{24,28},{28,32},{32,36}... | collective-permute-start | bytes 12296 | tf_op jit(solution)/shard_map/ppermute | solution.py:350
  8.2 24.6 %all-to-all-start = ((bf16[64,8,128]{2,1,0:T(8,128)(2,1)}), bf16[64,8,128]{2,1,0:T(8,128)(2,1)S(1)}, u32[]{:S(2)}, u32[]{:S(2)}) async-start(bf16[64,8,128]{2,1,0:T(8,128)(2,1)} %get-tuple-element.44), calls=%async_computation | async-start | bytes 262144 | tf_op jit(solution)/shard_map/all_to_all | solution.py:299
  33.5 7.1 %collective-permute-start.1 = (bf16[32,2048]{1,0:T(8,128)(2,1)S(1)}, bf16[32,2048]{1,0:T(8,128)(2,1)S(1)}, u32[]{:S(2)}, u32[]{:S(2)}) collective-permute-start(bf16[32,2048]{1,0:T(8,128)(2,1)S(1)} %get-tuple-element.52), channel_id=1, source_target_pairs={{0,1},{1,2},{2,3},{3,0},{4,5},{5,6},{6,7},{7,4},{8,9},{9,10},{10,1... | collective-permute-start | bytes 393224 | tf_op jit(solution)/shard_map/ppermute | solution.py:295
  34.9 5.8 %collective-permute-start.2 = (bf16[32,2048]{1,0:T(8,128)(2,1)S(1)}, bf16[32,2048]{1,0:T(8,128)(2,1)S(1)}, u32[]{:S(2)}, u32[]{:S(2)}) collective-permute-start(bf16[32,2048]{1,0:T(8,128)(2,1)S(1)} %get-tuple-element.53), channel_id=1, source_target_pairs={{0,3},{1,0},{2,1},{3,2},{4,7},{5,4},{6,5},{7,6},{8,11},{9,8},{10,9... | collective-permute-start | bytes 393224 | tf_op jit(solution)/shard_map/ppermute | solution.py:295
  36.4 7.1 %collective-permute-start.3 = (bf16[32,2048]{1,0:T(8,128)(2,1)S(1)}, bf16[32,2048]{1,0:T(8,128)(2,1)S(1)}, u32[]{:S(2)}, u32[]{:S(2)}) collective-permute-start(bf16[32,2048]{1,0:T(8,128)(2,1)S(1)} %get-tuple-element.54), channel_id=1, source_target_pairs={{0,2},{1,3},{2,0},{3,1},{4,6},{5,7},{6,4},{7,5},{8,10},{9,11},{10,... | collective-permute-start | bytes 393224 | tf_op jit(solution)/shard_map/ppermute | solution.py:295
  38.0 17.2 %collective-permute-start.4 = (bf16[2048,128]{1,0:T(8,128)(2,1)}, bf16[2048,128]{1,0:T(8,128)(2,1)}, u32[]{:S(2)}, u32[]{:S(2)}) collective-permute-start(bf16[2048,128]{1,0:T(8,128)(2,1)} %bitcast.17.g0), channel_id=1, source_target_pairs={{0,1},{1,2},{2,3},{3,0},{4,5},{5,6},{6,7},{7,4},{8,9},{9,10},{10,1... | collective-permute-start | bytes 1572872 | tf_op jit(solution)/shard_map/ppermute | solution.py:295
  38.4 16.9 %collective-permute-start.7 = (bf16[2048,128]{1,0:T(8,128)(2,1)}, bf16[2048,128]{1,0:T(8,128)(2,1)}, u32[]{:S(2)}, u32[]{:S(2)}) collective-permute-start(bf16[2048,128]{1,0:T(8,128)(2,1)} %bitcast.18.u0), channel_id=1, source_target_pairs={{0,3},{1,0},{2,1},{3,2},{4,7},{5,4},{6,5},{7,6},{8,11},{9,8},{10,9... | collective-permute-start | bytes 1572872 | tf_op jit(solution)/shard_map/ppermute | solution.py:295
  40.6 25.7 %collective-permute-start.10 = (bf16[128,2048]{1,0:T(8,128)(2,1)}, bf16[128,2048]{1,0:T(8,128)(2,1)S(1)}, u32[]{:S(2)}, u32[]{:S(2)}) collective-permute-start(bf16[128,2048]{1,0:T(8,128)(2,1)} %bitcast.19.d0), channel_id=1, source_target_pairs={{0,1},{1,2},{2,3},{3,0},{4,5},{5,6},{6,7},{7,4},{8,9},{9,10},{10,1... | collective-permute-start | bytes 1572872 | tf_op jit(solution)/shard_map/ppermute | solution.py:295
  44.9 44.7 %all-to-all-start.1 = ((bf16[64,2,2048]{2,1,0:T(2,128)(2,1)}), bf16[64,2,2048]{2,1,0:T(2,128)(2,1)S(1)}, u32[]{:S(2)}, u32[]{:S(2)}) async-start(bf16[64,2,2048]{2,1,0:T(2,128)(2,1)} %get-tuple-element.59), calls=%async_computation.1 | async-start | bytes 1048576 | tf_op jit(solution)/shard_map/all_to_all | solution.py:299
  51.1 15.3 %collective-permute-start.11 = (bf16[128,2048]{1,0:T(8,128)(2,1)}, bf16[128,2048]{1,0:T(8,128)(2,1)S(1)}, u32[]{:S(2)}, u32[]{:S(2)}) collective-permute-start(bf16[128,2048]{1,0:T(8,128)(2,1)} %bitcast.19.d0), channel_id=1, source_target_pairs={{0,3},{1,0},{2,1},{3,2},{4,7},{5,4},{6,5},{7,6},{8,11},{9,8},{10,9... | collective-permute-start | bytes 1572872 | tf_op jit(solution)/shard_map/ppermute | solution.py:295
  52.4 25.2 %collective-permute-start.5 = (bf16[2048,128]{1,0:T(8,128)(2,1)}, bf16[2048,128]{1,0:T(8,128)(2,1)S(1)}, u32[]{:S(2)}, u32[]{:S(2)}) collective-permute-start(bf16[2048,128]{1,0:T(8,128)(2,1)} %bitcast.18.u0), channel_id=1, source_target_pairs={{0,1},{1,2},{2,3},{3,0},{4,5},{5,6},{6,7},{7,4},{8,9},{9,10},{10,1... | collective-permute-start | bytes 1572872 | tf_op jit(solution)/shard_map/ppermute | solution.py:295
  55.2 27.6 %collective-permute-start.6 = (bf16[2048,128]{1,0:T(8,128)(2,1)}, bf16[2048,128]{1,0:T(8,128)(2,1)S(1)}, u32[]{:S(2)}, u32[]{:S(2)}) collective-permute-start(bf16[2048,128]{1,0:T(8,128)(2,1)} %bitcast.17.g0), channel_id=1, source_target_pairs={{0,3},{1,0},{2,1},{3,2},{4,7},{5,4},{6,5},{7,6},{8,11},{9,8},{10,9... | collective-permute-start | bytes 1572872 | tf_op jit(solution)/shard_map/ppermute | solution.py:295
  55.2 33.6 %collective-permute-start.8 = (bf16[2048,128]{1,0:T(8,128)(2,1)}, bf16[2048,128]{1,0:T(8,128)(2,1)S(1)}, u32[]{:S(2)}, u32[]{:S(2)}) collective-permute-start(bf16[2048,128]{1,0:T(8,128)(2,1)} %collective-permute-done.4.g1), channel_id=1, source_target_pairs={{0,1},{1,2},{2,3},{3,0},{4,5},{5,6},{6,7},{7,4},{8,9},{9,10},{10,1... | collective-permute-start | bytes 1572872 | tf_op jit(solution)/shard_map/ppermute | solution.py:295
  66.3 11.2 %copy-start = (bf16[128,2048]{1,0:T(8,128)(2,1)}, bf16[128,2048]{1,0:T(8,128)(2,1)S(1)}, u32[]{:S(2)}) copy-start(bf16[128,2048]{1,0:T(8,128)(2,1)S(1)} %collective-permute-done.10.d1) | copy-start | bytes 1572868
  66.3 23.3 %collective-permute-start.9 = (bf16[2048,128]{1,0:T(8,128)(2,1)}, bf16[2048,128]{1,0:T(8,128)(2,1)}, u32[]{:S(2)}, u32[]{:S(2)}) collective-permute-start(bf16[2048,128]{1,0:T(8,128)(2,1)} %collective-permute-done.7.u2), channel_id=1, source_target_pairs={{0,3},{1,0},{2,1},{3,2},{4,7},{5,4},{6,5},{7,6},{8,11},{9,8},{10,9... | collective-permute-start | bytes 1572872 | tf_op jit(solution)/shard_map/ppermute | solution.py:295
  66.4 11.2 %copy-start.1 = (bf16[128,2048]{1,0:T(8,128)(2,1)}, bf16[128,2048]{1,0:T(8,128)(2,1)S(1)}, u32[]{:S(2)}) copy-start(bf16[128,2048]{1,0:T(8,128)(2,1)S(1)} %collective-permute-done.11.d2) | copy-start | bytes 1572868
  66.4 28.1 %collective-permute-start.12 = (bf16[64,2048]{1,0:T(8,128)(2,1)S(1)}, bf16[64,2048]{1,0:T(8,128)(2,1)}, u32[]{:S(2)}, u32[]{:S(2)}) collective-permute-start(bf16[64,2048]{1,0:T(8,128)(2,1)S(1)} %slice.8), channel_id=1, source_target_pairs={{0,1},{1,2},{2,3},{3,0},{4,5},{5,6},{6,7},{7,4},{8,9},{9,10},{10,1... | collective-permute-start | bytes 786440 | tf_op jit(solution)/shard_map/ppermute | solution.py:295
  77.6 0.8 copy-start.4
  77.6 17.0 %collective-permute-start.13 = (bf16[64,2048]{1,0:T(8,128)(2,1)}, bf16[64,2048]{1,0:T(8,128)(2,1)}, u32[]{:S(2)}, u32[]{:S(2)}) collective-permute-start(bf16[64,2048]{1,0:T(8,128)(2,1)} %slice.9), channel_id=1, source_target_pairs={{0,3},{1,0},{2,1},{3,2},{4,7},{5,4},{6,5},{7,6},{8,11},{9,8},{10,9... | collective-permute-start | bytes 786440 | tf_op jit(solution)/shard_map/ppermute | solution.py:295
  82.8 6.0 %copy-start.2 = (bf16[2048,128]{1,0:T(8,128)(2,1)}, bf16[2048,128]{1,0:T(8,128)(2,1)S(1)}, u32[]{:S(2)}) copy-start(bf16[2048,128]{1,0:T(8,128)(2,1)S(1)} %collective-permute-done.6.g2) | copy-start | bytes 1572868
  88.8 0.8 copy-start.3

commit v2 on v1

--- a/solution.py
+++ b/solution.py
@@ -91,54 +91,71 @@
 
 
 def load_kernel(*refs):
-    count = (len(refs) - 2) // 2
-    far, near, edge, sems = refs[:count], refs[count : 2 * count], refs[-2], refs[-1]
-    copies = fetched(list(zip(far, near)), sems)
-    copies[0].wait()
-    edge[...] = near[0][near[0].shape[0] - edge.shape[0] :]
-    for copy in copies[1:]:
+    *far, extra, conv, small_pairs, large_pairs, rate, taps_wide, rows, taps, small_maps, large_maps, decay_param, wide, sems = refs
+    copies = fetched(list(zip(far, (rows, taps, small_maps, large_maps, decay_param, extra))), sems)
+    for copy in copies[:5]:
         copy.wait()
-
-
-def local_kernel(rows, taps, small_maps, large_maps, decay_param, extra, border, decays, states, totals, padded, maps):
     groups, half = decay_param.shape
     per_half = half // LANES
     step = groups * per_half
     length = rows.shape[0] // step
+    margin = wide.shape[0] - rows.shape[0]
     tap_count = taps.shape[0]
     tap_weights = taps[...].astype(F32)
-    rate = -8.0 * softplus(-decay_param[...])
-    margin = border.shape[0]
-    padded[0:margin] = border[...].astype(F32)
-    padded[margin:] = rows[...].astype(F32)
+    taps_wide[...] = tap_weights
+    rate[...] = -8.0 * softplus(-decay_param[...])
     head = small_maps.shape[-1]
     per_run = LANES // head
-    maps[...] = jnp.zeros(maps.shape, BF16)
+    small_pairs[...] = jnp.zeros(small_pairs.shape, BF16)
     for c in range(per_half):
         for m in range(2):
             for h in range(per_run):
                 at = h * head
-                maps[c, at : at + head, m * LANES + at : m * LANES + at + head] = small_maps[m, c * per_run + h]
+                small_pairs[c, at : at + head, m * LANES + at : m * LANES + at + head] = small_maps[m, c * per_run + h]
+            large_pairs[c, :, m * LANES : (m + 1) * LANES] = large_maps[m, c]
+    wide[0:margin] = jnp.zeros((margin, LANES), F32)
+    wide[margin:] = rows[...].astype(F32)
+    for run in range(step):
+        g, c = divmod(run, per_half)
+        at = slice(c * LANES, (c + 1) * LANES)
+        summed = None
+        for k in range(tap_count):
+            start = margin - (tap_count - 1 - k) * step + c * groups + g
+            term = tap_weights[k, g : g + 1, at] * wide[pl.ds(start, length, stride=step), :]
+            summed = term if summed is None else summed + term
+        conv[:, run * LANES : (run + 1) * LANES] = summed
+    copies[5].wait()
+
+
+def local_kernel(border, extra, conv, small_pairs, large_pairs, rate, taps, decays, states, totals, edge):
+    groups = rate.shape[0]
+    per_half = small_pairs.shape[0]
+    step = groups * per_half
+    length = conv.shape[0]
+    tap_count = taps.shape[0]
+    tap_weights = taps[...]
+    margin = border.shape[0]
+    edge[0:margin] = border[...].astype(F32)
+    edge[margin:] = jnp.zeros((edge.shape[0] - margin, LANES), F32)
+    top = (edge.shape[0] - margin) // step
     logs, ends = [], []
-    for g in range(groups):
-        for c in range(per_half):
-            at = slice(c * LANES, (c + 1) * LANES)
-            summed = None
-            for k in range(tap_count):
-                start = margin - (tap_count - 1 - k) * step + c * groups + g
-                term = tap_weights[k, g : g + 1, at] * padded[pl.ds(start, length, stride=step), :]
-                summed = term if summed is None else summed + term
-            conv_rows = summed.astype(BF16)
-            both = maps[c] if g == 0 else jnp.concatenate([large_maps[0, c], large_maps[1, c]], axis=1)
-            gates = jax.nn.sigmoid(dot(conv_rows, both))
-            log_decay = gates[:, :LANES] * rate[g : g + 1, at] + extra[pl.ds(c * groups + g, length, stride=step), :]
-            drive = jnp.sqrt(-expm1(2.0 * log_decay)) * gates[:, LANES:] * conv_rows.astype(F32)
-            product, state = chain_rows(jnp.exp(log_decay), drive)
-            to = slice((g * per_half + c) * LANES, (g * per_half + c + 1) * LANES)
-            decays[:, to] = product
-            states[:, to] = state
-            logs.append(jnp.sum(log_decay, axis=0, keepdims=True))
-            ends.append(state[length - 1 :])
+    for run in range(step):
+        g, c = divmod(run, per_half)
+        at = slice(c * LANES, (c + 1) * LANES)
+        to = slice(run * LANES, (run + 1) * LANES)
+        first = conv[0:top, to]
+        for k in range(tap_count - 1):
+            start = margin - (tap_count - 1 - k) * step + c * groups + g
+            first = first + tap_weights[k, g : g + 1, at] * edge[pl.ds(start, top, stride=step), :]
+        conv_rows = jnp.concatenate([first, conv[top:, to]], axis=0).astype(BF16)
+        gates = jax.nn.sigmoid(dot(conv_rows, (small_pairs, large_pairs)[g][c]))
+        log_decay = gates[:, :LANES] * rate[g : g + 1, at] + extra[pl.ds(c * groups + g, length, stride=step), :]
+        drive = jnp.sqrt(-expm1(2.0 * log_decay)) * gates[:, LANES:] * conv_rows.astype(F32)
+        product, state = chain_rows(jnp.exp(log_decay), drive)
+        decays[:, to] = product
+        states[:, to] = state
+        logs.append(jnp.sum(log_decay, axis=0, keepdims=True))
+        ends.append(state[length - 1 :])
     span = jnp.concatenate(logs + ends, axis=0).astype(BF16)
     for j in range(totals.shape[0]):
         totals[j] = span
@@ -333,6 +350,7 @@
 
     rows = flat(recurrence_input)
     margin = 16
+    border = lax.ppermute(rows[rows.shape[0] - margin :], "sp", [(i, i + 1) for i in range(sp_count - 1)])
     operands = (
         rows,
         convolution_taps,
@@ -341,13 +359,24 @@
         channel_decay,
         flat(position_log_extra),
     )
-    *operands, edge = kernel_call(
+    per_half = half // LANES
+    prepared = kernel_call(
         load_kernel,
-        [*(kept(x.shape, x.dtype) for x in operands), kept((margin, LANES), BF16)],
+        [
+            kept((rows.shape[0], LANES), F32),
+            kept((length, channels), F32),
+            kept((per_half, LANES, 2 * LANES), BF16),
+            kept((per_half, LANES, 2 * LANES), BF16),
+            kept((groups, half), F32),
+            kept(convolution_taps.shape, F32),
+        ],
         *((x, "hbm") for x in operands),
-        scratch=(pltpu.SemaphoreType.DMA((len(operands),)),),
-    )
-    border = lax.ppermute(edge, "sp", [(i, i + 1) for i in range(sp_count - 1)])
+        scratch=(
+            *(pltpu.VMEM(x.shape, x.dtype) for x in operands[:5]),
+            pltpu.VMEM((margin + rows.shape[0], LANES), F32),
+            pltpu.SemaphoreType.DMA((len(operands),)),
+        ),
+    )
 
     gate_w, up_w, down_w = routed_gate_weight[0], routed_up_weight[0], routed_down_weight[0]
     gate_left, up_right = turned(gate_w, 1), turned(up_w, -1)
@@ -358,11 +387,8 @@
     decays, states, totals = kernel_call(
         local_kernel,
         [kept((length, channels), F32), kept((length, channels), F32), shape((sp_count, 2 * runs, LANES), BF16)],
-        *((x, "vmem") for x in (*operands, border)),
-        scratch=(
-            pltpu.VMEM((margin + rows.shape[0], LANES), F32),
-            pltpu.VMEM((half // LANES, LANES, 2 * LANES), BF16),
-        ),
+        *((x, "vmem") for x in (border, *prepared)),
+        scratch=(pltpu.VMEM((margin + 8 * groups * per_half, LANES), F32),),
     )
     spans = swapped(totals, "sp")
 

time: 124 us -> 124 us (level)
  transfers between devices with their start and end apart: 16 -> 16, of which waited for: 8 -> 7; matrix products, arithmetic and copies ran while one was open for 1% -> 1% of each run, Pallas kernels for 9% -> 10%
where the time goes in v2:
time: 124 us; the launch traced here: 123 us
  waiting for transfers between devices  40.7 us (33%)
  starting transfers between devices  35.2 us (28%)
  blocking collectives  26.9 us (22%)
  Pallas kernels  17.3 us (14%)
  local copies, waits for them, and re-layouts  3.01 us (2%)
    ppermute x13, waiting for transfers between devices, turned(): lax.ppermute(shard, 'tp', [(i, (i + by) % count) for i in range(count)])  32.1 us
    all_to_all x1, blocking collectives, swapped(): return lax.all_to_all(pieces, axis, 0, 0, tiled=True)  26.9 us
    all_to_all x2, starting transfers between devices, swapped(): return lax.all_to_all(pieces, axis, 0, 0, tiled=True)  19.1 us
    pallas_call x9, Pallas kernels, kernel_call(): pl.pallas_call(body, out_shape=out_shape, in_specs=specs, out_specs=[VMEM...  17.3 us
    ppermute x13, starting transfers between devices, turned(): lax.ppermute(shard, 'tp', [(i, (i + by) % count) for i in range(count)])  11.7 us
    all_to_all x2, waiting for transfers between devices, swapped(): return lax.all_to_all(pieces, axis, 0, 0, tiled=True)  8.6 us
    ppermute x1, starting transfers between devices, shards(): lax.ppermute(rows[rows.shape[0] - margin:], 'sp', [(i, i + 1) for i in ra...  4.49 us
  transfers between devices with their start and end apart: 16, of which 7 were waited for; matrix products, arithmetic and copies ran while one was open for 1% of the time, Pallas kernels for 10%

profile of v2, /device:TPU:1, one launch (start us, length us, event | category | flops | bytes accessed | tf_op | source)
XLA Modules:
  0.0 123.3 jit_solution(12663333086548706464)
XLA Ops:
  0.0 0.7 slice.16
  0.7 4.5 %collective-permute-start = (bf16[16,128]{1,0:T(8,128)(2,1)S(1)}, bf16[16,128]{1,0:T(8,128)(2,1)S(1)}, u32[]{:S(2)}, u32[]{:S(2)}) collective-permute-start(bf16[16,128]{1,0:T(8,128)(2,1)S(1)} %bitcast.35), channel_id=1, source_target_pairs={{0,4},{4,8},{8,12},{12,16},{16,20},{20,24},{24,28},{28,32},{32,36}... | collective-permute-start | bytes 12296 | tf_op jit(solution)/shard_map/ppermute | solution.py:353
  5.2 1.4 %shard_map.199 = (f32[512,128]{1,0:T(8,128)S(1)}, f32[128,512]{1,0:T(8,128)S(1)}, bf16[2,128,256]{2,1,0:T(8,128)(2,1)S(1)}, bf16[2,128,256]{2,1,0:T(8,128)(2,1)S...) custom-call(bf16[512,128]{1,0:T(8,128)(2,1)} %bitcast.29, bf16[4,2,256]{2,1,0:T(2,128)(2,1)} %refs_1_.1, ...), custom_call_target="tpu_custom_call" | custom-call | tf_op jit(solution)/shard_map/pallas_call | solution.py:27
  6.5 0.0 collective-permute-done.border
  6.6 1.6 %shard_map.200 = (f32[128,512]{1,0:T(8,128)S(1)}, f32[128,512]{1,0:T(8,128)S(1)}, bf16[64,8,128]{2,1,0:T(8,128)(2,1)}) custom-call(bf16[16,128]{1,0:T(8,128)(2,1)S(1)} %collective-permute-done.border, f32[512,128]{1,0:T(8,128)S(1)} %get-tuple-element.36.extra, f32[128,512]{1,0:T(8,128)S(1)} %get-tuple-element.37.conv, ...), custom_call_target="tpu_custom_call" | custom-call | tf_op jit(solution)/shard_map/pallas_call | solution.py:27
  8.2 12.9 %all-to-all-start = ((bf16[64,8,128]{2,1,0:T(8,128)(2,1)}), bf16[64,8,128]{2,1,0:T(8,128)(2,1)S(1)}, u32[]{:S(2)}, u32[]{:S(2)}) async-start(bf16[64,8,128]{2,1,0:T(8,128)(2,1)} %get-tuple-element.42), calls=%async_computation | async-start | bytes 262144 | tf_op jit(solution)/shard_map/all_to_all | solution.py:316
  21.1 0.1 pad_add_fusion.places
  21.2 2.4 %shard_map.201 = (bf16[128,32]{1,0:T(8,128)(2,1)S(1)}, f32[32,128]{1,0:T(8,128)S(1)}, f32[128,512]{1,0:T(8,128)S(1)}, f32[128,512]{1,0:T(8,128)S(1)}, bf16[32,20...) custom-call(s32[2]{0:T(128)S(1)} %pad_add_fusion.places, ...), custom_call_target="tpu_custom_call" | custom-call | tf_op jit(solution)/shard_map/pallas_call | solution.py:27
  23.6 8.6 %all-to-all-done.spans = bf16[64,8,128]{2,1,0:T(8,128)(2,1)S(1)} async-done(((bf16[64,8,128]{2,1,0:T(8,128)(2,1)}), bf16[64,8,128]{2,1,0:T(8,128)(2,1)S(1)}, u32[]{:S(2)}, u32[]{:S(2)}) %all-to-all-start) | async-done | bytes 131104 | tf_op jit(solution)/shard_map/all_to_all | solution.py:316
  32.2 0.7 shard_map.202
  32.9 1.4 %collective-permute-start.1 = (bf16[32,2048]{1,0:T(8,128)(2,1)S(1)}, bf16[32,2048]{1,0:T(8,128)(2,1)S(1)}, u32[]{:S(2)}, u32[]{:S(2)}) collective-permute-start(bf16[32,2048]{1,0:T(8,128)(2,1)S(1)} %get-tuple-element.50), channel_id=1, source_target_pairs={{0,1},{1,2},{2,3},{3,0},{4,5},{5,6},{6,7},{7,4},{8,9},{9,10},{10,1... | collective-permute-start | bytes 393224 | tf_op jit(solution)/shard_map/ppermute | solution.py:312
  34.2 1.5 %collective-permute-start.2 = (bf16[32,2048]{1,0:T(8,128)(2,1)S(1)}, bf16[32,2048]{1,0:T(8,128)(2,1)S(1)}, u32[]{:S(2)}, u32[]{:S(2)}) collective-permute-start(bf16[32,2048]{1,0:T(8,128)(2,1)S(1)} %get-tuple-element.51), channel_id=1, source_target_pairs={{0,3},{1,0},{2,1},{3,2},{4,7},{5,4},{6,5},{7,6},{8,11},{9,8},{10,9... | collective-permute-start | bytes 393224 | tf_op jit(solution)/shard_map/ppermute | solution.py:312
  35.8 1.6 %collective-permute-start.3 = (bf16[32,2048]{1,0:T(8,128)(2,1)S(1)}, bf16[32,2048]{1,0:T(8,128)(2,1)S(1)}, u32[]{:S(2)}, u32[]{:S(2)}) collective-permute-start(bf16[32,2048]{1,0:T(8,128)(2,1)S(1)} %get-tuple-element.52), channel_id=1, source_target_pairs={{0,2},{1,3},{2,0},{3,1},{4,6},{5,7},{6,4},{7,5},{8,10},{9,11},{10,... | collective-permute-start | bytes 393224 | tf_op jit(solution)/shard_map/ppermute | solution.py:312
  37.3 0.4 collective-permute-start.4
  37.7 2.3 %collective-permute-start.7 = (bf16[2048,128]{1,0:T(8,128)(2,1)}, bf16[2048,128]{1,0:T(8,128)(2,1)}, u32[]{:S(2)}, u32[]{:S(2)}) collective-permute-start(bf16[2048,128]{1,0:T(8,128)(2,1)} %bitcast.20.u0), channel_id=1, source_target_pairs={{0,3},{1,0},{2,1},{3,2},{4,7},{5,4},{6,5},{7,6},{8,11},{9,8},{10,9... | collective-permute-start | bytes 1572872 | tf_op jit(solution)/shard_map/ppermute | solution.py:312
  40.0 0.0 collective-permute-done.1.refs_1_
  40.0 0.0 collective-permute-start.10
  40.0 0.0 collective-permute-done.2.refs_2_
  40.0 2.9 %collective-permute-done.3.refs_3_ = bf16[32,2048]{1,0:T(8,128)(2,1)S(1)} collective-permute-done((bf16[32,2048]{1,0:T(8,128)(2,1)S(1)}, bf16[32,2048]{1,0:T(8,128)(2,1)S(1)}, u32[]{:S(2)}, u32[]{:S(2)}) %collective-permute-start.3) | collective-permute-done | bytes 131104 | tf_op jit(solution)/shard_map/ppermute | solution.py:312
  42.9 1.4 %shard_map.203 = (bf16[32,2048]{1,0:T(8,128)(2,1)S(1)}, bf16[64,2,2048]{2,1,0:T(2,128)(2,1)}) custom-call(bf16[32,2048]{1,0:T(8,128)(2,1)S(1)} %get-tuple-element.49.refs_0_, bf16[32,2048]{1,0:T(8,128)(2,1)S(1)} %collective-permute-done.1.refs_1_, bf16[32,2048]{1,0:T(8,128)(2,1)S(1)} %collective-permute-done.2.refs_2_, ...), custom_call_target="tpu_custom_call" | custom-call | tf_op jit(solution)/shard_map/pallas_call | solution.py:27
  44.3 6.2 %all-to-all-start.1 = ((bf16[64,2,2048]{2,1,0:T(2,128)(2,1)}), bf16[64,2,2048]{2,1,0:T(2,128)(2,1)S(1)}, u32[]{:S(2)}, u32[]{:S(2)}) async-start(bf16[64,2,2048]{2,1,0:T(2,128)(2,1)} %get-tuple-element.57), calls=%async_computation.1 | async-start | bytes 1048576 | tf_op jit(solution)/shard_map/all_to_all | solution.py:316
  50.5 1.2 %collective-permute-start.11 = (bf16[128,2048]{1,0:T(8,128)(2,1)}, bf16[128,2048]{1,0:T(8,128)(2,1)S(1)}, u32[]{:S(2)}, u32[]{:S(2)}) collective-permute-start(bf16[128,2048]{1,0:T(8,128)(2,1)} %bitcast.21.d0), channel_id=1, source_target_pairs={{0,3},{1,0},{2,1},{3,2},{4,7},{5,4},{6,5},{7,6},{8,11},{9,8},{10,9... | collective-permute-start | bytes 1572872 | tf_op jit(solution)/shard_map/ppermute | solution.py:312
  51.7 0.3 collective-permute-start.5
  52.0 2.6 %collective-permute-done.4.g1 = bf16[2048,128]{1,0:T(8,128)(2,1)} collective-permute-done((bf16[2048,128]{1,0:T(8,128)(2,1)}, bf16[2048,128]{1,0:T(8,128)(2,1)}, u32[]{:S(2)}, u32[]{:S(2)}) %collective-permute-start.4) | collective-permute-done | bytes 524320 | tf_op jit(solution)/shard_map/ppermute | solution.py:312
  54.6 0.0 collective-permute-start.6
  54.6 0.0 collective-permute-done.7.u2
  54.6 1.5 %collective-permute-start.8 = (bf16[2048,128]{1,0:T(8,128)(2,1)}, bf16[2048,128]{1,0:T(8,128)(2,1)S(1)}, u32[]{:S(2)}, u32[]{:S(2)}) collective-permute-start(bf16[2048,128]{1,0:T(8,128)(2,1)} %collective-permute-done.4.g1), channel_id=1, source_target_pairs={{0,1},{1,2},{2,3},{3,0},{4,5},{5,6},{6,7},{7,4},{8,9},{9,10},{10,1... | collective-permute-start | bytes 1572872 | tf_op jit(solution)/shard_map/ppermute | solution.py:312
  56.0 9.7 %collective-permute-done.10.d1 = bf16[128,2048]{1,0:T(8,128)(2,1)S(1)} collective-permute-done((bf16[128,2048]{1,0:T(8,128)(2,1)}, bf16[128,2048]{1,0:T(8,128)(2,1)S(1)}, u32[]{:S(2)}, u32[]{:S(2)}) %collective-permute-start.10) | collective-permute-done | bytes 524320 | tf_op jit(solution)/shard_map/ppermute | solution.py:312
  65.7 0.0 copy-start
  65.7 0.0 collective-permute-start.9
  65.7 0.0 collective-permute-done.11.d2
  65.7 0.0 copy-start.1
  65.7 1.5 %collective-permute-start.12 = (bf16[64,2048]{1,0:T(8,128)(2,1)S(1)}, bf16[64,2048]{1,0:T(8,128)(2,1)}, u32[]{:S(2)}, u32[]{:S(2)}) collective-permute-start(bf16[64,2048]{1,0:T(8,128)(2,1)S(1)} %slice.17), channel_id=1, source_target_pairs={{0,1},{1,2},{2,3},{3,0},{4,5},{5,6},{6,7},{7,4},{8,9},{9,10},{10,1... | collective-permute-start | bytes 786440 | tf_op jit(solution)/shard_map/ppermute | solution.py:312
  67.3 0.7 slice.18
  68.0 8.9 %collective-permute-done.5.u1 = bf16[2048,128]{1,0:T(8,128)(2,1)S(1)} collective-permute-done((bf16[2048,128]{1,0:T(8,128)(2,1)}, bf16[2048,128]{1,0:T(8,128)(2,1)S(1)}, u32[]{:S(2)}, u32[]{:S(2)}) %collective-permute-start.5) | collective-permute-done | bytes 524320 | tf_op jit(solution)/shard_map/ppermute | solution.py:312
  76.9 0.0 copy-start.4
  76.9 0.0 collective-permute-start.13
  76.9 0.0 copy-done
  76.9 0.0 copy-done.1
  76.9 0.8 copy-done.4
  77.7 4.4 %shard_map.204 = (f32[32,2048]{1,0:T(8,128)S(1)}, f32[32,128]{1,0:T(8,128)S(1)}, f32[1,2048]{1,0:T(1,128)S(1)}, f32[1,2048]{1,0:T(1,128)S(1)}, bf16[2,2048,256]{2,1,0:T(8,128)(2,1)S(1)}) custom-call(bf16[32,2048]{1,0:T(8,128)(2,1)S(1)} %get-tuple-element.58.normed, bf16[2048,512]{1,0:T(8,128)(2,1)} %gate_w.1, bf16[2048,512]{1,0:T(8,128)(2,1)} %up_w.1, ...), custom_call_target="tpu_custom_call" | custom-call | tf_op jit(solution)/shard_map/pallas_call | solution.py:27
  82.2 0.0 collective-permute-done.6.g2
  82.2 0.0 copy-start.2
  82.2 6.0 %collective-permute-done.8.g3 = bf16[2048,128]{1,0:T(8,128)(2,1)S(1)} collective-permute-done((bf16[2048,128]{1,0:T(8,128)(2,1)}, bf16[2048,128]{1,0:T(8,128)(2,1)S(1)}, u32[]{:S(2)}, u32[]{:S(2)}) %collective-permute-start.8) | collective-permute-done | bytes 524320 | tf_op jit(solution)/shard_map/ppermute | solution.py:312
  88.2 0.0 copy-done.2
  88.2 0.0 copy-start.3
  88.2 0.8 copy-done.3
  89.0 0.0 collective-permute-done.9.u3
  89.0 0.0 all-to-all-done.1.rows
  89.0 2.9 %shard_map.205 = (f32[128,2048]{1,0:T(8,128)S(1)}, bf16[128,128]{1,0:T(8,128)(2,1)S(1)}) custom-call(bf16[64,2,2048]{2,1,0:T(2,128)(2,1)S(1)} %all-to-all-done.1.rows, bf16[2,2048,256]{2,1,0:T(8,128)(2,1)S(1)} %get-tuple-element.60.near, bf16[2048,128]{1,0:T(8,128)(2,1)} %copy-done.2, bf16[2048,128]{1,0:T(8,128)(2,1)} %collective-permute-done.7.u2, ...), custom_call_target="tpu_custom_call" | custom-call | tf_op jit(solution)/shard_map/pallas_call | solution.py:27
  91.8 2.1 %collective-permute-done.12.d3a = bf16[64,2048]{1,0:T(8,128)(2,1)} collective-permute-done((bf16[64,2048]{1,0:T(8,128)(2,1)S(1)}, bf16[64,2048]{1,0:T(8,128)(2,1)}, u32[]{:S(2)}, u32[]{:S(2)}) %collective-permute-start.12) | collective-permute-done | bytes 262176 | tf_op jit(solution)/shard_map/ppermute | solution.py:312
  93.9 0.0 collective-permute-done.13.d3b
  93.9 1.3 %shard_map.206 = bf16[64,2,2048]{2,1,0:T(2,128)(2,1)S(1)} custom-call(f32[128,2048]{1,0:T(8,128)S(1)} %get-tuple-element.61.acc, bf16[128,128]{1,0:T(8,128)(2,1)S(1)} %get-tuple-element.62.hidden, bf16[64,2048]{1,0:T(8,128)(2,1)} %collective-permute-done.12.d3a, bf16[64,2048]{1,0:T(8,128)(2,1)} %collective-permute-done.13.d3b), custom_call_target="tpu_custom_call" | custom-call | tf_op jit(solution)/shard_map/pallas_call | solution.py:27
  95.2 26.9 %all_to_all.15.returned = bf16[64,2,2048]{2,1,0:T(2,128)(2,1)S(1)} all-to-all(bf16[64,2,2048]{2,1,0:T(2,128)(2,1)S(1)} %shard_map.206), channel_id=1, replica_groups=mesh['sp'=64,'tp'=4] {'sp'}, dimensions={0} | all-to-all | bytes 1048576 | tf_op jit(solution)/shard_map/all_to_all | solution.py:316
  122.1 1.2 shard_map.207
  (1 shorter events, 0.0 us)
Async XLA Ops:
  0.7 5.9 %collective-permute-start = (bf16[16,128]{1,0:T(8,128)(2,1)S(1)}, bf16[16,128]{1,0:T(8,128)(2,1)S(1)}, u32[]{:S(2)}, u32[]{:S(2)}) collective-permute-start(bf16[16,128]{1,0:T(8,128)(2,1)S(1)} %bitcast.35), channel_id=1, source_target_pairs={{0,4},{4,8},{8,12},{12,16},{16,20},{20,24},{24,28},{28,32},{32,36}... | collective-permute-start | bytes 12296 | tf_op jit(solution)/shard_map/ppermute | solution.py:353
  8.2 24.0 %all-to-all-start = ((bf16[64,8,128]{2,1,0:T(8,128)(2,1)}), bf16[64,8,128]{2,1,0:T(8,128)(2,1)S(1)}, u32[]{:S(2)}, u32[]{:S(2)}) async-start(bf16[64,8,128]{2,1,0:T(8,128)(2,1)} %get-tuple-element.42), calls=%async_computation | async-start | bytes 262144 | tf_op jit(solution)/shard_map/all_to_all | solution.py:316
  32.9 7.1 %collective-permute-start.1 = (bf16[32,2048]{1,0:T(8,128)(2,1)S(1)}, bf16[32,2048]{1,0:T(8,128)(2,1)S(1)}, u32[]{:S(2)}, u32[]{:S(2)}) collective-permute-start(bf16[32,2048]{1,0:T(8,128)(2,1)S(1)} %get-tuple-element.50), channel_id=1, source_target_pairs={{0,1},{1,2},{2,3},{3,0},{4,5},{5,6},{6,7},{7,4},{8,9},{9,10},{10,1... | collective-permute-start | bytes 393224 | tf_op jit(solution)/shard_map/ppermute | solution.py:312
  34.2 5.8 %collective-permute-start.2 = (bf16[32,2048]{1,0:T(8,128)(2,1)S(1)}, bf16[32,2048]{1,0:T(8,128)(2,1)S(1)}, u32[]{:S(2)}, u32[]{:S(2)}) collective-permute-start(bf16[32,2048]{1,0:T(8,128)(2,1)S(1)} %get-tuple-element.51), channel_id=1, source_target_pairs={{0,3},{1,0},{2,1},{3,2},{4,7},{5,4},{6,5},{7,6},{8,11},{9,8},{10,9... | collective-permute-start | bytes 393224 | tf_op jit(solution)/shard_map/ppermute | solution.py:312
  35.8 7.1 %collective-permute-start.3 = (bf16[32,2048]{1,0:T(8,128)(2,1)S(1)}, bf16[32,2048]{1,0:T(8,128)(2,1)S(1)}, u32[]{:S(2)}, u32[]{:S(2)}) collective-permute-start(bf16[32,2048]{1,0:T(8,128)(2,1)S(1)} %get-tuple-element.52), channel_id=1, source_target_pairs={{0,2},{1,3},{2,0},{3,1},{4,6},{5,7},{6,4},{7,5},{8,10},{9,11},{10,... | collective-permute-start | bytes 393224 | tf_op jit(solution)/shard_map/ppermute | solution.py:312
  37.3 17.2 %collective-permute-start.4 = (bf16[2048,128]{1,0:T(8,128)(2,1)}, bf16[2048,128]{1,0:T(8,128)(2,1)}, u32[]{:S(2)}, u32[]{:S(2)}) collective-permute-start(bf16[2048,128]{1,0:T(8,128)(2,1)} %bitcast.19.g0), channel_id=1, source_target_pairs={{0,1},{1,2},{2,3},{3,0},{4,5},{5,6},{6,7},{7,4},{8,9},{9,10},{10,1... | collective-permute-start | bytes 1572872 | tf_op jit(solution)/shard_map/ppermute | solution.py:312
  37.7 16.9 %collective-permute-start.7 = (bf16[2048,128]{1,0:T(8,128)(2,1)}, bf16[2048,128]{1,0:T(8,128)(2,1)}, u32[]{:S(2)}, u32[]{:S(2)}) collective-permute-start(bf16[2048,128]{1,0:T(8,128)(2,1)} %bitcast.20.u0), channel_id=1, source_target_pairs={{0,3},{1,0},{2,1},{3,2},{4,7},{5,4},{6,5},{7,6},{8,11},{9,8},{10,9... | collective-permute-start | bytes 1572872 | tf_op jit(solution)/shard_map/ppermute | solution.py:312
  40.0 25.7 %collective-permute-start.10 = (bf16[128,2048]{1,0:T(8,128)(2,1)}, bf16[128,2048]{1,0:T(8,128)(2,1)S(1)}, u32[]{:S(2)}, u32[]{:S(2)}) collective-permute-start(bf16[128,2048]{1,0:T(8,128)(2,1)} %bitcast.21.d0), channel_id=1, source_target_pairs={{0,1},{1,2},{2,3},{3,0},{4,5},{5,6},{6,7},{7,4},{8,9},{9,10},{10,1... | collective-permute-start | bytes 1572872 | tf_op jit(solution)/shard_map/ppermute | solution.py:312
  44.3 44.7 %all-to-all-start.1 = ((bf16[64,2,2048]{2,1,0:T(2,128)(2,1)}), bf16[64,2,2048]{2,1,0:T(2,128)(2,1)S(1)}, u32[]{:S(2)}, u32[]{:S(2)}) async-start(bf16[64,2,2048]{2,1,0:T(2,128)(2,1)} %get-tuple-element.57), calls=%async_computation.1 | async-start | bytes 1048576 | tf_op jit(solution)/shard_map/all_to_all | solution.py:316
  50.5 15.3 %collective-permute-start.11 = (bf16[128,2048]{1,0:T(8,128)(2,1)}, bf16[128,2048]{1,0:T(8,128)(2,1)S(1)}, u32[]{:S(2)}, u32[]{:S(2)}) collective-permute-start(bf16[128,2048]{1,0:T(8,128)(2,1)} %bitcast.21.d0), channel_id=1, source_target_pairs={{0,3},{1,0},{2,1},{3,2},{4,7},{5,4},{6,5},{7,6},{8,11},{9,8},{10,9... | collective-permute-start | bytes 1572872 | tf_op jit(solution)/shard_map/ppermute | solution.py:312
  51.7 25.2 %collective-permute-start.5 = (bf16[2048,128]{1,0:T(8,128)(2,1)}, bf16[2048,128]{1,0:T(8,128)(2,1)S(1)}, u32[]{:S(2)}, u32[]{:S(2)}) collective-permute-start(bf16[2048,128]{1,0:T(8,128)(2,1)} %bitcast.20.u0), channel_id=1, source_target_pairs={{0,1},{1,2},{2,3},{3,0},{4,5},{5,6},{6,7},{7,4},{8,9},{9,10},{10,1... | collective-permute-start | bytes 1572872 | tf_op jit(solution)/shard_map/ppermute | solution.py:312
  54.6 27.6 %collective-permute-start.6 = (bf16[2048,128]{1,0:T(8,128)(2,1)}, bf16[2048,128]{1,0:T(8,128)(2,1)S(1)}, u32[]{:S(2)}, u32[]{:S(2)}) collective-permute-start(bf16[2048,128]{1,0:T(8,128)(2,1)} %bitcast.19.g0), channel_id=1, source_target_pairs={{0,3},{1,0},{2,1},{3,2},{4,7},{5,4},{6,5},{7,6},{8,11},{9,8},{10,9... | collective-permute-start | bytes 1572872 | tf_op jit(solution)/shard_map/ppermute | solution.py:312
  54.6 33.6 %collective-permute-start.8 = (bf16[2048,128]{1,0:T(8,128)(2,1)}, bf16[2048,128]{1,0:T(8,128)(2,1)S(1)}, u32[]{:S(2)}, u32[]{:S(2)}) collective-permute-start(bf16[2048,128]{1,0:T(8,128)(2,1)} %collective-permute-done.4.g1), channel_id=1, source_target_pairs={{0,1},{1,2},{2,3},{3,0},{4,5},{5,6},{6,7},{7,4},{8,9},{9,10},{10,1... | collective-permute-start | bytes 1572872 | tf_op jit(solution)/shard_map/ppermute | solution.py:312
  65.7 11.2 %copy-start = (bf16[128,2048]{1,0:T(8,128)(2,1)}, bf16[128,2048]{1,0:T(8,128)(2,1)S(1)}, u32[]{:S(2)}) copy-start(bf16[128,2048]{1,0:T(8,128)(2,1)S(1)} %collective-permute-done.10.d1) | copy-start | bytes 1572868
  65.7 23.3 %collective-permute-start.9 = (bf16[2048,128]{1,0:T(8,128)(2,1)}, bf16[2048,128]{1,0:T(8,128)(2,1)}, u32[]{:S(2)}, u32[]{:S(2)}) collective-permute-start(bf16[2048,128]{1,0:T(8,128)(2,1)} %collective-permute-done.7.u2), channel_id=1, source_target_pairs={{0,3},{1,0},{2,1},{3,2},{4,7},{5,4},{6,5},{7,6},{8,11},{9,8},{10,9... | collective-permute-start | bytes 1572872 | tf_op jit(solution)/shard_map/ppermute | solution.py:312
  65.7 11.2 %copy-start.1 = (bf16[128,2048]{1,0:T(8,128)(2,1)}, bf16[128,2048]{1,0:T(8,128)(2,1)S(1)}, u32[]{:S(2)}) copy-start(bf16[128,2048]{1,0:T(8,128)(2,1)S(1)} %collective-permute-done.11.d2) | copy-start | bytes 1572868
  65.7 28.1 %collective-permute-start.12 = (bf16[64,2048]{1,0:T(8,128)(2,1)S(1)}, bf16[64,2048]{1,0:T(8,128)(2,1)}, u32[]{:S(2)}, u32[]{:S(2)}) collective-permute-start(bf16[64,2048]{1,0:T(8,128)(2,1)S(1)} %slice.17), channel_id=1, source_target_pairs={{0,1},{1,2},{2,3},{3,0},{4,5},{5,6},{6,7},{7,4},{8,9},{9,10},{10,1... | collective-permute-start | bytes 786440 | tf_op jit(solution)/shard_map/ppermute | solution.py:312
  76.9 0.8 copy-start.4
  76.9 17.0 %collective-permute-start.13 = (bf16[64,2048]{1,0:T(8,128)(2,1)}, bf16[64,2048]{1,0:T(8,128)(2,1)}, u32[]{:S(2)}, u32[]{:S(2)}) collective-permute-start(bf16[64,2048]{1,0:T(8,128)(2,1)} %slice.18), channel_id=1, source_target_pairs={{0,3},{1,0},{2,1},{3,2},{4,7},{5,4},{6,5},{7,6},{8,11},{9,8},{10,9... | collective-permute-start | bytes 786440 | tf_op jit(solution)/shard_map/ppermute | solution.py:312
  82.2 6.0 %copy-start.2 = (bf16[2048,128]{1,0:T(8,128)(2,1)}, bf16[2048,128]{1,0:T(8,128)(2,1)S(1)}, u32[]{:S(2)}) copy-start(bf16[2048,128]{1,0:T(8,128)(2,1)S(1)} %collective-permute-done.6.g2) | copy-start | bytes 1572868
  88.2 0.8 copy-start.3

commit v3 on v1

--- a/solution.py
+++ b/solution.py
@@ -239,9 +239,9 @@
     return moves
 
 
-def shared_kernel(normed, gate_w, up_w, down_w, merge, gain, bias, g0, u0, g1, u1, base, *rest):
+def shared_kernel(normed, gate_w, up_w, down_w, merge, gain, bias, g0, u0, base, *rest):
     *kept, near, sems = rest
-    copies = fetched(pair_moves(near, ((g0, u0), (g1, u1))), sems)
+    copies = fetched(pair_moves(near, ((g0, u0),)), sems)
     for target, source in zip(kept, (merge, gain, bias)):
         target[...] = source[...]
     rows = normed[...]
@@ -252,8 +252,8 @@
         copy.wait()
 
 
-def expert_kernel(rows, near, g2, u2, g3, u3, d0, d1, d2, acc, last, far, down, sems):
-    moves = pair_moves(far, ((g2, u2), (g3, u3)))
+def expert_kernel(rows, near, g1, u1, g2, u2, g3, u3, d0, d1, d2, acc, last, far, down, sems):
+    moves = pair_moves(far, ((g1, u1), (g2, u2), (g3, u3)))
     unit = d0.shape[0]
     moves += [(piece, down.at[j * unit : (j + 1) * unit]) for j, piece in enumerate((d0, d1, d2))]
     copies = fetched(moves, sems)
@@ -425,7 +425,7 @@
     down_far = turned(down_left[:cut], 1), turned(down_right[cut:], -1)
 
     last = (merge, second_norm_gain.reshape(1, width), second_norm_bias.reshape(1, width))
-    near_weights = (gate_w, up_w, gate_left, up_left)
+    near_weights = (gate_w, up_w)
     unit = gate_w.shape[1]
     base, *last, near = kernel_call(
         shared_kernel,
@@ -443,7 +443,7 @@
         *((w, "hbm") for w in near_weights),
         scratch=(pltpu.SemaphoreType.DMA((len(near_weights),)),),
     )
-    weights = (gate_right, up_right, gate_far, up_far, down_w, down_left, down_right)
+    weights = (gate_left, up_left, gate_right, up_right, gate_far, up_far, down_w, down_left, down_right)
     acc, hidden = kernel_call(
         expert_kernel,
         [kept((slot_count, width), F32), kept((slot_count, unit), BF16)],
@@ -451,13 +451,17 @@
         (near, "vmem"),
         *((w, "hbm") for w in weights),
         scratch=(
-            pltpu.VMEM((2, width, 2 * unit), BF16),
+            pltpu.VMEM((tp_count - 1, width, 2 * unit), BF16),
             pltpu.VMEM((3 * unit, width), BF16),
             pltpu.SemaphoreType.DMA((len(weights),)),
         ),
     )
     leaving = kernel_call(
-        last_kernel, kept((expert_count, SLOTS, width), BF16), (acc, "vmem"), (hidden, "vmem"), *down_far
+        last_kernel,
+        kept((expert_count, SLOTS, width), BF16),
+        (acc, "vmem"),
+        (hidden, "vmem"),
+        *((w, "vmem") for w in down_far),
     )
     returned = swapped(leaving, "sp")
     return kernel_call(

time: 124 us -> 123 us (level)
  no operation moved by 1% of the time
where the time goes in v3:
time: 123 us
  waiting for transfers between devices  41.2 us (33%)
  starting transfers between devices  35.9 us (29%)
  blocking collectives  26.9 us (22%)
  Pallas kernels  16.4 us (13%)
  local copies, waits for them, and re-layouts  2.32 us (2%)
    ppermute x13, waiting for transfers between devices, turned(): lax.ppermute(shard, 'tp', [(i, (i + by) % count) for i in range(count)])  31.8 us
    all_to_all x1, blocking collectives, swapped(): return lax.all_to_all(pieces, axis, 0, 0, tiled=True)  26.9 us
    all_to_all x2, starting transfers between devices, swapped(): return lax.all_to_all(pieces, axis, 0, 0, tiled=True)  19.7 us
    pallas_call x9, Pallas kernels, kernel_call(): pl.pallas_call(body, out_shape=out_shape, in_specs=specs, out_specs=[VMEM...  16.4 us
    ppermute x13, starting transfers between devices, turned(): lax.ppermute(shard, 'tp', [(i, (i + by) % count) for i in range(count)])  11.7 us
    all_to_all x2, waiting for transfers between devices, swapped(): return lax.all_to_all(pieces, axis, 0, 0, tiled=True)  8.6 us
    ppermute x1, starting transfers between devices, shards(): border = lax.ppermute(edge, 'sp', [(i, i + 1) for i in range(sp_count - 1)])  4.5 us
  transfers between devices with their start and end apart: 16, of which 8 were waited for; matrix products, arithmetic and copies ran while one was open for 1% of the time, Pallas kernels for 9%

profile of v3, /device:TPU:1, one launch (start us, length us, event | category | flops | bytes accessed | tf_op | source)
XLA Modules:
  0.0 122.9 jit_solution(513758085024407016)
XLA Ops:
  0.0 1.2 %shard_map.199 = (bf16[512,128]{1,0:T(8,128)(2,1)S(1)}, bf16[4,2,256]{2,1,0:T(2,128)(2,1)S(1)}, bf16[2,4,64,64]{3,2,1,0:T(8,128)(2,1)S(1)}, bf16[2,2,128,128]{3,...) custom-call(bf16[512,128]{1,0:T(8,128)(2,1)} %bitcast.27, ...), custom_call_target="tpu_custom_call" | custom-call | tf_op jit(solution)/shard_map/pallas_call | solution.py:27
  1.2 4.5 %collective-permute-start = (bf16[16,128]{1,0:T(8,128)(2,1)S(1)}, bf16[16,128]{1,0:T(8,128)(2,1)S(1)}, u32[]{:S(2)}, u32[]{:S(2)}) collective-permute-start(bf16[16,128]{1,0:T(8,128)(2,1)S(1)} %get-tuple-element.43), channel_id=1, source_target_pairs={{0,4},{4,8},{8,12},{12,16},{16,20},{20,24},{24,28},{28,32},{32,36}... | collective-permute-start | bytes 12296 | tf_op jit(solution)/shard_map/ppermute | solution.py:350
  5.7 0.7 collective-permute-done.border
  6.5 1.7 %shard_map.200 = (f32[128,512]{1,0:T(8,128)S(1)}, f32[128,512]{1,0:T(8,128)S(1)}, bf16[64,8,128]{2,1,0:T(8,128)(2,1)}) custom-call(bf16[512,128]{1,0:T(8,128)(2,1)S(1)} %get-tuple-element.37.rows, bf16[4,2,256]{2,1,0:T(2,128)(2,1)S(1)} %get-tuple-element.38.taps, bf16[2,4,64,64]{3,2,1,0:T(8,128)(2,1)S(1)} %get-tuple-element.39.small_maps, ...), custom_call_target="tpu_custom_call" | custom-call | tf_op jit(solution)/shard_map/pallas_call | solution.py:27
  8.2 13.5 %all-to-all-start = ((bf16[64,8,128]{2,1,0:T(8,128)(2,1)}), bf16[64,8,128]{2,1,0:T(8,128)(2,1)S(1)}, u32[]{:S(2)}, u32[]{:S(2)}) async-start(bf16[64,8,128]{2,1,0:T(8,128)(2,1)} %get-tuple-element.44), calls=%async_computation | async-start | bytes 262144 | tf_op jit(solution)/shard_map/all_to_all | solution.py:299
  21.8 0.1 pad_add_fusion.places
  21.8 2.4 %shard_map.201 = (bf16[128,32]{1,0:T(8,128)(2,1)S(1)}, f32[32,128]{1,0:T(8,128)S(1)}, f32[128,512]{1,0:T(8,128)S(1)}, f32[128,512]{1,0:T(8,128)S(1)}, bf16[32,20...) custom-call(s32[2]{0:T(128)S(1)} %pad_add_fusion.places, ...), custom_call_target="tpu_custom_call" | custom-call | tf_op jit(solution)/shard_map/pallas_call | solution.py:27
  24.2 8.6 %all-to-all-done.spans = bf16[64,8,128]{2,1,0:T(8,128)(2,1)S(1)} async-done(((bf16[64,8,128]{2,1,0:T(8,128)(2,1)}), bf16[64,8,128]{2,1,0:T(8,128)(2,1)S(1)}, u32[]{:S(2)}, u32[]{:S(2)}) %all-to-all-start) | async-done | bytes 131104 | tf_op jit(solution)/shard_map/all_to_all | solution.py:299
  32.8 0.7 shard_map.202
  33.5 1.4 %collective-permute-start.1 = (bf16[32,2048]{1,0:T(8,128)(2,1)S(1)}, bf16[32,2048]{1,0:T(8,128)(2,1)S(1)}, u32[]{:S(2)}, u32[]{:S(2)}) collective-permute-start(bf16[32,2048]{1,0:T(8,128)(2,1)S(1)} %get-tuple-element.52), channel_id=1, source_target_pairs={{0,1},{1,2},{2,3},{3,0},{4,5},{5,6},{6,7},{7,4},{8,9},{9,10},{10,1... | collective-permute-start | bytes 393224 | tf_op jit(solution)/shard_map/ppermute | solution.py:295
  34.9 1.5 %collective-permute-start.2 = (bf16[32,2048]{1,0:T(8,128)(2,1)S(1)}, bf16[32,2048]{1,0:T(8,128)(2,1)S(1)}, u32[]{:S(2)}, u32[]{:S(2)}) collective-permute-start(bf16[32,2048]{1,0:T(8,128)(2,1)S(1)} %get-tuple-element.53), channel_id=1, source_target_pairs={{0,3},{1,0},{2,1},{3,2},{4,7},{5,4},{6,5},{7,6},{8,11},{9,8},{10,9... | collective-permute-start | bytes 393224 | tf_op jit(solution)/shard_map/ppermute | solution.py:295
  36.4 1.6 %collective-permute-start.3 = (bf16[32,2048]{1,0:T(8,128)(2,1)S(1)}, bf16[32,2048]{1,0:T(8,128)(2,1)S(1)}, u32[]{:S(2)}, u32[]{:S(2)}) collective-permute-start(bf16[32,2048]{1,0:T(8,128)(2,1)S(1)} %get-tuple-element.54), channel_id=1, source_target_pairs={{0,2},{1,3},{2,0},{3,1},{4,6},{5,7},{6,4},{7,5},{8,10},{9,11},{10,... | collective-permute-start | bytes 393224 | tf_op jit(solution)/shard_map/ppermute | solution.py:295
  38.0 0.4 collective-permute-start.4
  38.4 2.3 %collective-permute-start.7 = (bf16[2048,128]{1,0:T(8,128)(2,1)}, bf16[2048,128]{1,0:T(8,128)(2,1)}, u32[]{:S(2)}, u32[]{:S(2)}) collective-permute-start(bf16[2048,128]{1,0:T(8,128)(2,1)} %bitcast.18.u0), channel_id=1, source_target_pairs={{0,3},{1,0},{2,1},{3,2},{4,7},{5,4},{6,5},{7,6},{8,11},{9,8},{10,9... | collective-permute-start | bytes 1572872 | tf_op jit(solution)/shard_map/ppermute | solution.py:295
  40.6 0.0 collective-permute-done.1.refs_1_
  40.6 0.0 collective-permute-start.10
  40.6 0.0 collective-permute-done.2.refs_2_
  40.7 2.9 %collective-permute-done.3.refs_3_ = bf16[32,2048]{1,0:T(8,128)(2,1)S(1)} collective-permute-done((bf16[32,2048]{1,0:T(8,128)(2,1)S(1)}, bf16[32,2048]{1,0:T(8,128)(2,1)S(1)}, u32[]{:S(2)}, u32[]{:S(2)}) %collective-permute-start.3) | collective-permute-done | bytes 131104 | tf_op jit(solution)/shard_map/ppermute | solution.py:295
  43.5 1.4 %shard_map.203 = (bf16[32,2048]{1,0:T(8,128)(2,1)S(1)}, bf16[64,2,2048]{2,1,0:T(2,128)(2,1)}) custom-call(bf16[32,2048]{1,0:T(8,128)(2,1)S(1)} %get-tuple-element.51.refs_0_, bf16[32,2048]{1,0:T(8,128)(2,1)S(1)} %collective-permute-done.1.refs_1_, bf16[32,2048]{1,0:T(8,128)(2,1)S(1)} %collective-permute-done.2.refs_2_, ...), custom_call_target="tpu_custom_call" | custom-call | tf_op jit(solution)/shard_map/pallas_call | solution.py:27
  44.9 6.2 %all-to-all-start.1 = ((bf16[64,2,2048]{2,1,0:T(2,128)(2,1)}), bf16[64,2,2048]{2,1,0:T(2,128)(2,1)S(1)}, u32[]{:S(2)}, u32[]{:S(2)}) async-start(bf16[64,2,2048]{2,1,0:T(2,128)(2,1)} %get-tuple-element.59), calls=%async_computation.1 | async-start | bytes 1048576 | tf_op jit(solution)/shard_map/all_to_all | solution.py:299
  51.1 1.3 %collective-permute-start.11 = (bf16[128,2048]{1,0:T(8,128)(2,1)}, bf16[128,2048]{1,0:T(8,128)(2,1)S(1)}, u32[]{:S(2)}, u32[]{:S(2)}) collective-permute-start(bf16[128,2048]{1,0:T(8,128)(2,1)} %bitcast.19.d0), channel_id=1, source_target_pairs={{0,3},{1,0},{2,1},{3,2},{4,7},{5,4},{6,5},{7,6},{8,11},{9,8},{10,9... | collective-permute-start | bytes 1572872 | tf_op jit(solution)/shard_map/ppermute | solution.py:295
  52.4 0.3 collective-permute-start.5
  52.7 2.6 %collective-permute-done.4.g1 = bf16[2048,128]{1,0:T(8,128)(2,1)} collective-permute-done((bf16[2048,128]{1,0:T(8,128)(2,1)}, bf16[2048,128]{1,0:T(8,128)(2,1)}, u32[]{:S(2)}, u32[]{:S(2)}) %collective-permute-start.4) | collective-permute-done | bytes 524320 | tf_op jit(solution)/shard_map/ppermute | solution.py:295
  55.2 0.0 collective-permute-start.6
  55.2 0.0 collective-permute-done.7.u2
  55.2 1.5 %collective-permute-start.8 = (bf16[2048,128]{1,0:T(8,128)(2,1)}, bf16[2048,128]{1,0:T(8,128)(2,1)S(1)}, u32[]{:S(2)}, u32[]{:S(2)}) collective-permute-start(bf16[2048,128]{1,0:T(8,128)(2,1)} %collective-permute-done.4.g1), channel_id=1, source_target_pairs={{0,1},{1,2},{2,3},{3,0},{4,5},{5,6},{6,7},{7,4},{8,9},{9,10},{10,1... | collective-permute-start | bytes 1572872 | tf_op jit(solution)/shard_map/ppermute | solution.py:295
  56.7 9.7 %collective-permute-done.10.d1 = bf16[128,2048]{1,0:T(8,128)(2,1)S(1)} collective-permute-done((bf16[128,2048]{1,0:T(8,128)(2,1)}, bf16[128,2048]{1,0:T(8,128)(2,1)S(1)}, u32[]{:S(2)}, u32[]{:S(2)}) %collective-permute-start.10) | collective-permute-done | bytes 524320 | tf_op jit(solution)/shard_map/ppermute | solution.py:295
  66.3 0.0 copy-start
  66.3 0.0 collective-permute-start.9
  66.4 0.0 collective-permute-done.11.d2
  66.4 0.0 copy-start.1
  66.4 1.5 %collective-permute-start.12 = (bf16[64,2048]{1,0:T(8,128)(2,1)S(1)}, bf16[64,2048]{1,0:T(8,128)(2,1)S(1)}, u32[]{:S(2)}, u32[]{:S(2)}) collective-permute-start(bf16[64,2048]{1,0:T(8,128)(2,1)S(1)} %slice.8), channel_id=1, source_target_pairs={{0,1},{1,2},{2,3},{3,0},{4,5},{5,6},{6,7},{7,4},{8,9},{9,10},{10,1... | collective-permute-start | bytes 786440 | tf_op jit(solution)/shard_map/ppermute | solution.py:295
  67.9 0.7 slice.9
  68.6 8.9 %collective-permute-done.5.u1 = bf16[2048,128]{1,0:T(8,128)(2,1)S(1)} collective-permute-done((bf16[2048,128]{1,0:T(8,128)(2,1)}, bf16[2048,128]{1,0:T(8,128)(2,1)S(1)}, u32[]{:S(2)}, u32[]{:S(2)}) %collective-permute-start.5) | collective-permute-done | bytes 524320 | tf_op jit(solution)/shard_map/ppermute | solution.py:295
  77.6 0.0 copy-start.2
  77.6 0.0 collective-permute-start.13
  77.6 0.0 copy-done.1
  77.6 0.8 copy-done.2
  78.4 4.2 %shard_map.204 = (f32[32,2048]{1,0:T(8,128)S(1)}, f32[32,128]{1,0:T(8,128)S(1)}, f32[1,2048]{1,0:T(1,128)S(1)}, f32[1,2048]{1,0:T(1,128)S(1)}, bf16[1,2048,256]{2,1,0:T(8,128)(2,1)S(1)}) custom-call(bf16[32,2048]{1,0:T(8,128)(2,1)S(1)} %get-tuple-element.60.normed, bf16[2048,512]{1,0:T(8,128)(2,1)} %gate_w.1, bf16[2048,512]{1,0:T(8,128)(2,1)} %up_w.1, ...), custom_call_target="tpu_custom_call" | custom-call | tf_op jit(solution)/shard_map/pallas_call | solution.py:27
  82.5 0.0 copy-done
  82.5 0.0 collective-permute-done.6.g2
  82.6 0.0 copy-start.3
  82.6 6.2 %collective-permute-done.8.g3 = bf16[2048,128]{1,0:T(8,128)(2,1)S(1)} collective-permute-done((bf16[2048,128]{1,0:T(8,128)(2,1)}, bf16[2048,128]{1,0:T(8,128)(2,1)S(1)}, u32[]{:S(2)}, u32[]{:S(2)}) %collective-permute-start.8) | collective-permute-done | bytes 524320 | tf_op jit(solution)/shard_map/ppermute | solution.py:295
  88.8 0.0 copy-done.3
  88.8 0.0 copy-start.4
  88.8 0.8 copy-done.4
  89.6 0.0 collective-permute-done.9.u3
  89.6 0.0 all-to-all-done.1.rows
  89.6 3.3 %shard_map.205 = (f32[128,2048]{1,0:T(8,128)S(1)}, bf16[128,128]{1,0:T(8,128)(2,1)S(1)}) custom-call(bf16[64,2,2048]{2,1,0:T(2,128)(2,1)S(1)} %all-to-all-done.1.rows, bf16[1,2048,256]{2,1,0:T(8,128)(2,1)S(1)} %get-tuple-element.62.near, bf16[2048,128]{1,0:T(8,128)(2,1)} %collective-permute-done.4.g1, bf16[2048,128]{1,0:T(8,128)(2,1)} %copy-done.2, ...), custom_call_target="tpu_custom_call" | custom-call | tf_op jit(solution)/shard_map/pallas_call | solution.py:27
  92.9 1.6 %collective-permute-done.12.d3a = bf16[64,2048]{1,0:T(8,128)(2,1)S(1)} collective-permute-done((bf16[64,2048]{1,0:T(8,128)(2,1)S(1)}, bf16[64,2048]{1,0:T(8,128)(2,1)S(1)}, u32[]{:S(2)}, u32[]{:S(2)}) %collective-permute-start.12) | collective-permute-done | bytes 262176 | tf_op jit(solution)/shard_map/ppermute | solution.py:295
  94.4 0.0 collective-permute-done.13.d3b
  94.4 0.3 shard_map.206
  94.7 26.9 %all_to_all.15.returned = bf16[64,2,2048]{2,1,0:T(2,128)(2,1)S(1)} all-to-all(bf16[64,2,2048]{2,1,0:T(2,128)(2,1)S(1)} %shard_map.206), channel_id=1, replica_groups=mesh['sp'=64,'tp'=4] {'sp'}, dimensions={0} | all-to-all | bytes 1048576 | tf_op jit(solution)/shard_map/all_to_all | solution.py:299
  121.6 1.2 shard_map.207
  (1 shorter events, 0.0 us)
Async XLA Ops:
  1.2 5.2 %collective-permute-start = (bf16[16,128]{1,0:T(8,128)(2,1)S(1)}, bf16[16,128]{1,0:T(8,128)(2,1)S(1)}, u32[]{:S(2)}, u32[]{:S(2)}) collective-permute-start(bf16[16,128]{1,0:T(8,128)(2,1)S(1)} %get-tuple-element.43), channel_id=1, source_target_pairs={{0,4},{4,8},{8,12},{12,16},{16,20},{20,24},{24,28},{28,32},{32,36}... | collective-permute-start | bytes 12296 | tf_op jit(solution)/shard_map/ppermute | solution.py:350
  8.2 24.6 %all-to-all-start = ((bf16[64,8,128]{2,1,0:T(8,128)(2,1)}), bf16[64,8,128]{2,1,0:T(8,128)(2,1)S(1)}, u32[]{:S(2)}, u32[]{:S(2)}) async-start(bf16[64,8,128]{2,1,0:T(8,128)(2,1)} %get-tuple-element.44), calls=%async_computation | async-start | bytes 262144 | tf_op jit(solution)/shard_map/all_to_all | solution.py:299
  33.5 7.1 %collective-permute-start.1 = (bf16[32,2048]{1,0:T(8,128)(2,1)S(1)}, bf16[32,2048]{1,0:T(8,128)(2,1)S(1)}, u32[]{:S(2)}, u32[]{:S(2)}) collective-permute-start(bf16[32,2048]{1,0:T(8,128)(2,1)S(1)} %get-tuple-element.52), channel_id=1, source_target_pairs={{0,1},{1,2},{2,3},{3,0},{4,5},{5,6},{6,7},{7,4},{8,9},{9,10},{10,1... | collective-permute-start | bytes 393224 | tf_op jit(solution)/shard_map/ppermute | solution.py:295
  34.9 5.8 %collective-permute-start.2 = (bf16[32,2048]{1,0:T(8,128)(2,1)S(1)}, bf16[32,2048]{1,0:T(8,128)(2,1)S(1)}, u32[]{:S(2)}, u32[]{:S(2)}) collective-permute-start(bf16[32,2048]{1,0:T(8,128)(2,1)S(1)} %get-tuple-element.53), channel_id=1, source_target_pairs={{0,3},{1,0},{2,1},{3,2},{4,7},{5,4},{6,5},{7,6},{8,11},{9,8},{10,9... | collective-permute-start | bytes 393224 | tf_op jit(solution)/shard_map/ppermute | solution.py:295
  36.4 7.1 %collective-permute-start.3 = (bf16[32,2048]{1,0:T(8,128)(2,1)S(1)}, bf16[32,2048]{1,0:T(8,128)(2,1)S(1)}, u32[]{:S(2)}, u32[]{:S(2)}) collective-permute-start(bf16[32,2048]{1,0:T(8,128)(2,1)S(1)} %get-tuple-element.54), channel_id=1, source_target_pairs={{0,2},{1,3},{2,0},{3,1},{4,6},{5,7},{6,4},{7,5},{8,10},{9,11},{10,... | collective-permute-start | bytes 393224 | tf_op jit(solution)/shard_map/ppermute | solution.py:295
  38.0 17.2 %collective-permute-start.4 = (bf16[2048,128]{1,0:T(8,128)(2,1)}, bf16[2048,128]{1,0:T(8,128)(2,1)}, u32[]{:S(2)}, u32[]{:S(2)}) collective-permute-start(bf16[2048,128]{1,0:T(8,128)(2,1)} %bitcast.17.g0), channel_id=1, source_target_pairs={{0,1},{1,2},{2,3},{3,0},{4,5},{5,6},{6,7},{7,4},{8,9},{9,10},{10,1... | collective-permute-start | bytes 1572872 | tf_op jit(solution)/shard_map/ppermute | solution.py:295
  38.4 16.9 %collective-permute-start.7 = (bf16[2048,128]{1,0:T(8,128)(2,1)}, bf16[2048,128]{1,0:T(8,128)(2,1)}, u32[]{:S(2)}, u32[]{:S(2)}) collective-permute-start(bf16[2048,128]{1,0:T(8,128)(2,1)} %bitcast.18.u0), channel_id=1, source_target_pairs={{0,3},{1,0},{2,1},{3,2},{4,7},{5,4},{6,5},{7,6},{8,11},{9,8},{10,9... | collective-permute-start | bytes 1572872 | tf_op jit(solution)/shard_map/ppermute | solution.py:295
  40.6 25.7 %collective-permute-start.10 = (bf16[128,2048]{1,0:T(8,128)(2,1)}, bf16[128,2048]{1,0:T(8,128)(2,1)S(1)}, u32[]{:S(2)}, u32[]{:S(2)}) collective-permute-start(bf16[128,2048]{1,0:T(8,128)(2,1)} %bitcast.19.d0), channel_id=1, source_target_pairs={{0,1},{1,2},{2,3},{3,0},{4,5},{5,6},{6,7},{7,4},{8,9},{9,10},{10,1... | collective-permute-start | bytes 1572872 | tf_op jit(solution)/shard_map/ppermute | solution.py:295
  44.9 44.7 %all-to-all-start.1 = ((bf16[64,2,2048]{2,1,0:T(2,128)(2,1)}), bf16[64,2,2048]{2,1,0:T(2,128)(2,1)S(1)}, u32[]{:S(2)}, u32[]{:S(2)}) async-start(bf16[64,2,2048]{2,1,0:T(2,128)(2,1)} %get-tuple-element.59), calls=%async_computation.1 | async-start | bytes 1048576 | tf_op jit(solution)/shard_map/all_to_all | solution.py:299
  51.1 15.3 %collective-permute-start.11 = (bf16[128,2048]{1,0:T(8,128)(2,1)}, bf16[128,2048]{1,0:T(8,128)(2,1)S(1)}, u32[]{:S(2)}, u32[]{:S(2)}) collective-permute-start(bf16[128,2048]{1,0:T(8,128)(2,1)} %bitcast.19.d0), channel_id=1, source_target_pairs={{0,3},{1,0},{2,1},{3,2},{4,7},{5,4},{6,5},{7,6},{8,11},{9,8},{10,9... | collective-permute-start | bytes 1572872 | tf_op jit(solution)/shard_map/ppermute | solution.py:295
  52.4 25.2 %collective-permute-start.5 = (bf16[2048,128]{1,0:T(8,128)(2,1)}, bf16[2048,128]{1,0:T(8,128)(2,1)S(1)}, u32[]{:S(2)}, u32[]{:S(2)}) collective-permute-start(bf16[2048,128]{1,0:T(8,128)(2,1)} %bitcast.18.u0), channel_id=1, source_target_pairs={{0,1},{1,2},{2,3},{3,0},{4,5},{5,6},{6,7},{7,4},{8,9},{9,10},{10,1... | collective-permute-start | bytes 1572872 | tf_op jit(solution)/shard_map/ppermute | solution.py:295
  55.2 27.3 %collective-permute-start.6 = (bf16[2048,128]{1,0:T(8,128)(2,1)}, bf16[2048,128]{1,0:T(8,128)(2,1)S(1)}, u32[]{:S(2)}, u32[]{:S(2)}) collective-permute-start(bf16[2048,128]{1,0:T(8,128)(2,1)} %bitcast.17.g0), channel_id=1, source_target_pairs={{0,3},{1,0},{2,1},{3,2},{4,7},{5,4},{6,5},{7,6},{8,11},{9,8},{10,9... | collective-permute-start | bytes 1572872 | tf_op jit(solution)/shard_map/ppermute | solution.py:295
  55.2 33.6 %collective-permute-start.8 = (bf16[2048,128]{1,0:T(8,128)(2,1)}, bf16[2048,128]{1,0:T(8,128)(2,1)S(1)}, u32[]{:S(2)}, u32[]{:S(2)}) collective-permute-start(bf16[2048,128]{1,0:T(8,128)(2,1)} %collective-permute-done.4.g1), channel_id=1, source_target_pairs={{0,1},{1,2},{2,3},{3,0},{4,5},{5,6},{6,7},{7,4},{8,9},{9,10},{10,1... | collective-permute-start | bytes 1572872 | tf_op jit(solution)/shard_map/ppermute | solution.py:295
  66.3 16.2 %copy-start = (bf16[128,2048]{1,0:T(8,128)(2,1)}, bf16[128,2048]{1,0:T(8,128)(2,1)S(1)}, u32[]{:S(2)}) copy-start(bf16[128,2048]{1,0:T(8,128)(2,1)S(1)} %collective-permute-done.10.d1) | copy-start | bytes 1572868
  66.3 23.3 %collective-permute-start.9 = (bf16[2048,128]{1,0:T(8,128)(2,1)}, bf16[2048,128]{1,0:T(8,128)(2,1)}, u32[]{:S(2)}, u32[]{:S(2)}) collective-permute-start(bf16[2048,128]{1,0:T(8,128)(2,1)} %collective-permute-done.7.u2), channel_id=1, source_target_pairs={{0,3},{1,0},{2,1},{3,2},{4,7},{5,4},{6,5},{7,6},{8,11},{9,8},{10,9... | collective-permute-start | bytes 1572872 | tf_op jit(solution)/shard_map/ppermute | solution.py:295
  66.4 11.2 %copy-start.1 = (bf16[128,2048]{1,0:T(8,128)(2,1)}, bf16[128,2048]{1,0:T(8,128)(2,1)S(1)}, u32[]{:S(2)}) copy-start(bf16[128,2048]{1,0:T(8,128)(2,1)S(1)} %collective-permute-done.11.d2) | copy-start | bytes 1572868
  66.4 28.0 %collective-permute-start.12 = (bf16[64,2048]{1,0:T(8,128)(2,1)S(1)}, bf16[64,2048]{1,0:T(8,128)(2,1)S(1)}, u32[]{:S(2)}, u32[]{:S(2)}) collective-permute-start(bf16[64,2048]{1,0:T(8,128)(2,1)S(1)} %slice.8), channel_id=1, source_target_pairs={{0,1},{1,2},{2,3},{3,0},{4,5},{5,6},{6,7},{7,4},{8,9},{9,10},{10,1... | collective-permute-start | bytes 786440 | tf_op jit(solution)/shard_map/ppermute | solution.py:295
  77.6 0.8 copy-start.2
  77.6 16.9 %collective-permute-start.13 = (bf16[64,2048]{1,0:T(8,128)(2,1)}, bf16[64,2048]{1,0:T(8,128)(2,1)S(1)}, u32[]{:S(2)}, u32[]{:S(2)}) collective-permute-start(bf16[64,2048]{1,0:T(8,128)(2,1)} %slice.9), channel_id=1, source_target_pairs={{0,3},{1,0},{2,1},{3,2},{4,7},{5,4},{6,5},{7,6},{8,11},{9,8},{10,9... | collective-permute-start | bytes 786440 | tf_op jit(solution)/shard_map/ppermute | solution.py:295
  82.6 6.3 %copy-start.3 = (bf16[2048,128]{1,0:T(8,128)(2,1)}, bf16[2048,128]{1,0:T(8,128)(2,1)S(1)}, u32[]{:S(2)}) copy-start(bf16[2048,128]{1,0:T(8,128)(2,1)S(1)} %collective-permute-done.6.g2) | copy-start | bytes 1572868
  88.8 0.8 copy-start.4

commit v4 on v3

--- a/solution.py
+++ b/solution.py
@@ -239,9 +239,9 @@
     return moves
 
 
-def shared_kernel(normed, gate_w, up_w, down_w, merge, gain, bias, g0, u0, base, *rest):
-    *kept, near, sems = rest
-    copies = fetched(pair_moves(near, ((g0, u0),)), sems)
+def shared_kernel(normed, gate_w, up_w, down_w, merge, gain, bias, g0, u0, d0, base, *rest):
+    *kept, near, near_down, sems = rest
+    copies = fetched(pair_moves(near, ((g0, u0),)) + [(d0, near_down)], sems)
     for target, source in zip(kept, (merge, gain, bias)):
         target[...] = source[...]
     rows = normed[...]
@@ -252,10 +252,10 @@
         copy.wait()
 
 
-def expert_kernel(rows, near, g1, u1, g2, u2, g3, u3, d0, d1, d2, acc, last, far, down, sems):
+def expert_kernel(rows, near, near_down, g1, u1, g2, u2, g3, u3, d1, d2, acc, last, far, down, sems):
     moves = pair_moves(far, ((g1, u1), (g2, u2), (g3, u3)))
-    unit = d0.shape[0]
-    moves += [(piece, down.at[j * unit : (j + 1) * unit]) for j, piece in enumerate((d0, d1, d2))]
+    unit = d2.shape[0]
+    moves += [(piece, down.at[j * unit : (j + 1) * unit]) for j, piece in enumerate((d1, d2))]
     copies = fetched(moves, sems)
     picked = rows[...].reshape(-1, rows.shape[-1])
 
@@ -271,7 +271,7 @@
     last[...] = hidden.pop()
     for copy in copies[2 * far.shape[0] :]:
         copy.wait()
-    acc[...] = dot(jnp.concatenate(hidden, axis=1), down[...])
+    acc[...] = dot(hidden[0], near_down[...]) + dot(jnp.concatenate(hidden[1:], axis=1), down[...])
 
 
 def last_kernel(acc, hidden, d3a, d3b, out):
@@ -425,14 +425,15 @@
     down_far = turned(down_left[:cut], 1), turned(down_right[cut:], -1)
 
     last = (merge, second_norm_gain.reshape(1, width), second_norm_bias.reshape(1, width))
-    near_weights = (gate_w, up_w)
+    near_weights = (gate_w, up_w, down_w)
     unit = gate_w.shape[1]
-    base, *last, near = kernel_call(
+    base, *last, near, near_down = kernel_call(
         shared_kernel,
         [
             kept((quarter, width), F32),
             *(kept(x.shape, F32) for x in last),
-            kept((len(near_weights) // 2, width, 2 * unit), BF16),
+            kept((1, width, 2 * unit), BF16),
+            kept((unit, width), BF16),
         ],
         (normed, "vmem"),
         shared_gate_weight,
@@ -443,16 +444,17 @@
         *((w, "hbm") for w in near_weights),
         scratch=(pltpu.SemaphoreType.DMA((len(near_weights),)),),
     )
-    weights = (gate_left, up_left, gate_right, up_right, gate_far, up_far, down_w, down_left, down_right)
+    weights = (gate_left, up_left, gate_right, up_right, gate_far, up_far, down_left, down_right)
     acc, hidden = kernel_call(
         expert_kernel,
         [kept((slot_count, width), F32), kept((slot_count, unit), BF16)],
         (arrived, "vmem"),
         (near, "vmem"),
+        (near_down, "vmem"),
         *((w, "hbm") for w in weights),
         scratch=(
             pltpu.VMEM((tp_count - 1, width, 2 * unit), BF16),
-            pltpu.VMEM((3 * unit, width), BF16),
+            pltpu.VMEM((2 * unit, width), BF16),
             pltpu.SemaphoreType.DMA((len(weights),)),
         ),
     )

time: 123 us -> 123 us (level)
  no operation moved by 1% of the time
where the time goes in v4:
time: 123 us
  waiting for transfers between devices  41.1 us (33%)
  starting transfers between devices  35.1 us (29%)
  blocking collectives  26.9 us (22%)
  Pallas kernels  16.5 us (13%)
  local copies, waits for them, and re-layouts  3.09 us (3%)
    ppermute x13, waiting for transfers between devices, turned(): lax.ppermute(shard, 'tp', [(i, (i + by) % count) for i in range(count)])  31.7 us
    all_to_all x1, blocking collectives, swapped(): return lax.all_to_all(pieces, axis, 0, 0, tiled=True)  26.9 us
    all_to_all x2, starting transfers between devices, swapped(): return lax.all_to_all(pieces, axis, 0, 0, tiled=True)  19.7 us
    pallas_call x9, Pallas kernels, kernel_call(): pl.pallas_call(body, out_shape=out_shape, in_specs=specs, out_specs=[VMEM...  16.5 us
    ppermute x13, starting transfers between devices, turned(): lax.ppermute(shard, 'tp', [(i, (i + by) % count) for i in range(count)])  10.9 us
    all_to_all x2, waiting for transfers between devices, swapped(): return lax.all_to_all(pieces, axis, 0, 0, tiled=True)  8.6 us
    ppermute x1, starting transfers between devices, shards(): border = lax.ppermute(edge, 'sp', [(i, i + 1) for i in range(sp_count - 1)])  4.5 us
  transfers between devices with their start and end apart: 16, of which 8 were waited for; matrix products, arithmetic and copies ran while one was open for 1% of the time, Pallas kernels for 9%

profile of v4, /device:TPU:1, one launch (start us, length us, event | category | flops | bytes accessed | tf_op | source)
XLA Modules:
  0.0 122.9 jit_solution(10584944152567117058)
XLA Ops:
  0.0 1.2 %shard_map.199 = (bf16[512,128]{1,0:T(8,128)(2,1)S(1)}, bf16[4,2,256]{2,1,0:T(2,128)(2,1)S(1)}, bf16[2,4,64,64]{3,2,1,0:T(8,128)(2,1)S(1)}, bf16[2,2,128,128]{3,...) custom-call(bf16[512,128]{1,0:T(8,128)(2,1)} %bitcast.27, ...), custom_call_target="tpu_custom_call" | custom-call | tf_op jit(solution)/shard_map/pallas_call | solution.py:27
  1.2 4.5 %collective-permute-start = (bf16[16,128]{1,0:T(8,128)(2,1)S(1)}, bf16[16,128]{1,0:T(8,128)(2,1)S(1)}, u32[]{:S(2)}, u32[]{:S(2)}) collective-permute-start(bf16[16,128]{1,0:T(8,128)(2,1)S(1)} %get-tuple-element.44), channel_id=1, source_target_pairs={{0,4},{4,8},{8,12},{12,16},{16,20},{20,24},{24,28},{28,32},{32,36}... | collective-permute-start | bytes 12296 | tf_op jit(solution)/shard_map/ppermute | solution.py:350
  5.7 0.7 collective-permute-done.border
  6.5 1.7 %shard_map.200 = (f32[128,512]{1,0:T(8,128)S(1)}, f32[128,512]{1,0:T(8,128)S(1)}, bf16[64,8,128]{2,1,0:T(8,128)(2,1)}) custom-call(bf16[512,128]{1,0:T(8,128)(2,1)S(1)} %get-tuple-element.38.rows, bf16[4,2,256]{2,1,0:T(2,128)(2,1)S(1)} %get-tuple-element.39.taps, bf16[2,4,64,64]{3,2,1,0:T(8,128)(2,1)S(1)} %get-tuple-element.40.small_maps, ...), custom_call_target="tpu_custom_call" | custom-call | tf_op jit(solution)/shard_map/pallas_call | solution.py:27
  8.2 13.5 %all-to-all-start = ((bf16[64,8,128]{2,1,0:T(8,128)(2,1)}), bf16[64,8,128]{2,1,0:T(8,128)(2,1)S(1)}, u32[]{:S(2)}, u32[]{:S(2)}) async-start(bf16[64,8,128]{2,1,0:T(8,128)(2,1)} %get-tuple-element.45), calls=%async_computation | async-start | bytes 262144 | tf_op jit(solution)/shard_map/all_to_all | solution.py:299
  21.8 0.1 pad_add_fusion.places
  21.8 2.4 %shard_map.201 = (bf16[128,32]{1,0:T(8,128)(2,1)S(1)}, f32[32,128]{1,0:T(8,128)S(1)}, f32[128,512]{1,0:T(8,128)S(1)}, f32[128,512]{1,0:T(8,128)S(1)}, bf16[32,20...) custom-call(s32[2]{0:T(128)S(1)} %pad_add_fusion.places, ...), custom_call_target="tpu_custom_call" | custom-call | tf_op jit(solution)/shard_map/pallas_call | solution.py:27
  24.2 8.6 %all-to-all-done.spans = bf16[64,8,128]{2,1,0:T(8,128)(2,1)S(1)} async-done(((bf16[64,8,128]{2,1,0:T(8,128)(2,1)}), bf16[64,8,128]{2,1,0:T(8,128)(2,1)S(1)}, u32[]{:S(2)}, u32[]{:S(2)}) %all-to-all-start) | async-done | bytes 131104 | tf_op jit(solution)/shard_map/all_to_all | solution.py:299
  32.8 0.7 shard_map.202
  33.5 1.4 %collective-permute-start.1 = (bf16[32,2048]{1,0:T(8,128)(2,1)S(1)}, bf16[32,2048]{1,0:T(8,128)(2,1)S(1)}, u32[]{:S(2)}, u32[]{:S(2)}) collective-permute-start(bf16[32,2048]{1,0:T(8,128)(2,1)S(1)} %get-tuple-element.53), channel_id=1, source_target_pairs={{0,1},{1,2},{2,3},{3,0},{4,5},{5,6},{6,7},{7,4},{8,9},{9,10},{10,1... | collective-permute-start | bytes 393224 | tf_op jit(solution)/shard_map/ppermute | solution.py:295
  34.9 1.5 %collective-permute-start.2 = (bf16[32,2048]{1,0:T(8,128)(2,1)S(1)}, bf16[32,2048]{1,0:T(8,128)(2,1)S(1)}, u32[]{:S(2)}, u32[]{:S(2)}) collective-permute-start(bf16[32,2048]{1,0:T(8,128)(2,1)S(1)} %get-tuple-element.54), channel_id=1, source_target_pairs={{0,3},{1,0},{2,1},{3,2},{4,7},{5,4},{6,5},{7,6},{8,11},{9,8},{10,9... | collective-permute-start | bytes 393224 | tf_op jit(solution)/shard_map/ppermute | solution.py:295
  36.4 1.6 %collective-permute-start.3 = (bf16[32,2048]{1,0:T(8,128)(2,1)S(1)}, bf16[32,2048]{1,0:T(8,128)(2,1)S(1)}, u32[]{:S(2)}, u32[]{:S(2)}) collective-permute-start(bf16[32,2048]{1,0:T(8,128)(2,1)S(1)} %get-tuple-element.55), channel_id=1, source_target_pairs={{0,2},{1,3},{2,0},{3,1},{4,6},{5,7},{6,4},{7,5},{8,10},{9,11},{10,... | collective-permute-start | bytes 393224 | tf_op jit(solution)/shard_map/ppermute | solution.py:295
  38.0 0.4 collective-permute-start.4
  38.4 2.3 %collective-permute-start.7 = (bf16[2048,128]{1,0:T(8,128)(2,1)}, bf16[2048,128]{1,0:T(8,128)(2,1)}, u32[]{:S(2)}, u32[]{:S(2)}) collective-permute-start(bf16[2048,128]{1,0:T(8,128)(2,1)} %bitcast.18.u0), channel_id=1, source_target_pairs={{0,3},{1,0},{2,1},{3,2},{4,7},{5,4},{6,5},{7,6},{8,11},{9,8},{10,9... | collective-permute-start | bytes 1572872 | tf_op jit(solution)/shard_map/ppermute | solution.py:295
  40.6 0.0 collective-permute-done.1.refs_1_
  40.6 0.0 collective-permute-start.10
  40.6 0.0 collective-permute-done.2.refs_2_
  40.7 2.9 %collective-permute-done.3.refs_3_ = bf16[32,2048]{1,0:T(8,128)(2,1)S(1)} collective-permute-done((bf16[32,2048]{1,0:T(8,128)(2,1)S(1)}, bf16[32,2048]{1,0:T(8,128)(2,1)S(1)}, u32[]{:S(2)}, u32[]{:S(2)}) %collective-permute-start.3) | collective-permute-done | bytes 131104 | tf_op jit(solution)/shard_map/ppermute | solution.py:295
  43.5 1.4 %shard_map.203 = (bf16[32,2048]{1,0:T(8,128)(2,1)S(1)}, bf16[64,2,2048]{2,1,0:T(2,128)(2,1)}) custom-call(bf16[32,2048]{1,0:T(8,128)(2,1)S(1)} %get-tuple-element.52.refs_0_, bf16[32,2048]{1,0:T(8,128)(2,1)S(1)} %collective-permute-done.1.refs_1_, bf16[32,2048]{1,0:T(8,128)(2,1)S(1)} %collective-permute-done.2.refs_2_, ...), custom_call_target="tpu_custom_call" | custom-call | tf_op jit(solution)/shard_map/pallas_call | solution.py:27
  44.9 6.2 %all-to-all-start.1 = ((bf16[64,2,2048]{2,1,0:T(2,128)(2,1)}), bf16[64,2,2048]{2,1,0:T(2,128)(2,1)S(1)}, u32[]{:S(2)}, u32[]{:S(2)}) async-start(bf16[64,2,2048]{2,1,0:T(2,128)(2,1)} %get-tuple-element.60), calls=%async_computation.1 | async-start | bytes 1048576 | tf_op jit(solution)/shard_map/all_to_all | solution.py:299
  51.1 1.3 %collective-permute-start.11 = (bf16[128,2048]{1,0:T(8,128)(2,1)}, bf16[128,2048]{1,0:T(8,128)(2,1)S(1)}, u32[]{:S(2)}, u32[]{:S(2)}) collective-permute-start(bf16[128,2048]{1,0:T(8,128)(2,1)} %bitcast.19.d0), channel_id=1, source_target_pairs={{0,3},{1,0},{2,1},{3,2},{4,7},{5,4},{6,5},{7,6},{8,11},{9,8},{10,9... | collective-permute-start | bytes 1572872 | tf_op jit(solution)/shard_map/ppermute | solution.py:295
  52.4 0.3 collective-permute-start.5
  52.7 2.6 %collective-permute-done.4.g1 = bf16[2048,128]{1,0:T(8,128)(2,1)} collective-permute-done((bf16[2048,128]{1,0:T(8,128)(2,1)}, bf16[2048,128]{1,0:T(8,128)(2,1)}, u32[]{:S(2)}, u32[]{:S(2)}) %collective-permute-start.4) | collective-permute-done | bytes 524320 | tf_op jit(solution)/shard_map/ppermute | solution.py:295
  55.2 0.0 collective-permute-start.6
  55.2 0.0 collective-permute-done.7.u2
  55.2 1.5 %collective-permute-start.8 = (bf16[2048,128]{1,0:T(8,128)(2,1)}, bf16[2048,128]{1,0:T(8,128)(2,1)S(1)}, u32[]{:S(2)}, u32[]{:S(2)}) collective-permute-start(bf16[2048,128]{1,0:T(8,128)(2,1)} %collective-permute-done.4.g1), channel_id=1, source_target_pairs={{0,1},{1,2},{2,3},{3,0},{4,5},{5,6},{6,7},{7,4},{8,9},{9,10},{10,1... | collective-permute-start | bytes 1572872 | tf_op jit(solution)/shard_map/ppermute | solution.py:295
  56.7 9.7 %collective-permute-done.10.d1 = bf16[128,2048]{1,0:T(8,128)(2,1)S(1)} collective-permute-done((bf16[128,2048]{1,0:T(8,128)(2,1)}, bf16[128,2048]{1,0:T(8,128)(2,1)S(1)}, u32[]{:S(2)}, u32[]{:S(2)}) %collective-permute-start.10) | collective-permute-done | bytes 524320 | tf_op jit(solution)/shard_map/ppermute | solution.py:295
  66.3 0.0 copy-start
  66.3 0.0 collective-permute-start.9
  66.4 0.8 copy-done
  67.1 0.0 collective-permute-done.11.d2
  67.1 0.0 copy-start.1
  67.1 0.8 collective-permute-start.12
  67.9 0.7 slice.9
  68.7 8.9 %collective-permute-done.5.u1 = bf16[2048,128]{1,0:T(8,128)(2,1)S(1)} collective-permute-done((bf16[2048,128]{1,0:T(8,128)(2,1)}, bf16[2048,128]{1,0:T(8,128)(2,1)S(1)}, u32[]{:S(2)}, u32[]{:S(2)}) %collective-permute-start.5) | collective-permute-done | bytes 524320 | tf_op jit(solution)/shard_map/ppermute | solution.py:295
  77.6 0.0 copy-start.2
  77.6 0.0 collective-permute-start.13
  77.6 0.0 copy-done.1
  77.6 0.8 copy-done.2
  78.4 4.3 %shard_map.204 = (f32[32,2048]{1,0:T(8,128)S(1)}, f32[32,128]{1,0:T(8,128)S(1)}, f32[1,2048]{1,0:T(1,128)S(1)}, f32[1,2048]{1,0:T(1,128)S(1)}, bf16[1,2048,256]{...) custom-call(bf16[32,2048]{1,0:T(8,128)(2,1)S(1)} %get-tuple-element.61.normed, bf16[2048,512]{1,0:T(8,128)(2,1)} %gate_w.1, ...), custom_call_target="tpu_custom_call" | custom-call | tf_op jit(solution)/shard_map/pallas_call | solution.py:27
  82.7 0.0 collective-permute-done.6.g2
  82.7 0.0 copy-start.3
  82.7 6.1 %collective-permute-done.8.g3 = bf16[2048,128]{1,0:T(8,128)(2,1)S(1)} collective-permute-done((bf16[2048,128]{1,0:T(8,128)(2,1)}, bf16[2048,128]{1,0:T(8,128)(2,1)S(1)}, u32[]{:S(2)}, u32[]{:S(2)}) %collective-permute-start.8) | collective-permute-done | bytes 524320 | tf_op jit(solution)/shard_map/ppermute | solution.py:295
  88.8 0.0 copy-done.3
  88.8 0.0 copy-start.4
  88.8 0.8 copy-done.4
  89.6 0.0 collective-permute-done.9.u3
  89.6 0.0 all-to-all-done.1.rows
  89.6 3.3 %shard_map.205 = (f32[128,2048]{1,0:T(8,128)S(1)}, bf16[128,128]{1,0:T(8,128)(2,1)S(1)}) custom-call(bf16[64,2,2048]{2,1,0:T(2,128)(2,1)S(1)} %all-to-all-done.1.rows, bf16[1,2048,256]{2,1,0:T(8,128)(2,1)S(1)} %get-tuple-element.63.near, bf16[128,2048]{1,0:T(8,128)(2,1)S(1)} %get-tuple-element.64.near_down, bf16[2048,128]{1,0:T(8,128)(2,1)} %collective-permute-done.4.g1, ...), custom_call_target="tpu_custom_call" | custom-call | tf_op jit(solution)/shard_map/pallas_call | solution.py:27
  92.9 1.6 %collective-permute-done.12.d3a = bf16[64,2048]{1,0:T(8,128)(2,1)S(1)} collective-permute-done((bf16[64,2048]{1,0:T(8,128)(2,1)S(1)}, bf16[64,2048]{1,0:T(8,128)(2,1)S(1)}, u32[]{:S(2)}, u32[]{:S(2)}) %collective-permute-start.12) | collective-permute-done | bytes 262176 | tf_op jit(solution)/shard_map/ppermute | solution.py:295
  94.4 0.0 collective-permute-done.13.d3b
  94.4 0.3 shard_map.206
  94.7 26.9 %all_to_all.15.returned = bf16[64,2,2048]{2,1,0:T(2,128)(2,1)S(1)} all-to-all(bf16[64,2,2048]{2,1,0:T(2,128)(2,1)S(1)} %shard_map.206), channel_id=1, replica_groups=mesh['sp'=64,'tp'=4] {'sp'}, dimensions={0} | all-to-all | bytes 1048576 | tf_op jit(solution)/shard_map/all_to_all | solution.py:299
  121.6 1.2 shard_map.207
  (1 shorter events, 0.0 us)
Async XLA Ops:
  1.2 5.2 %collective-permute-start = (bf16[16,128]{1,0:T(8,128)(2,1)S(1)}, bf16[16,128]{1,0:T(8,128)(2,1)S(1)}, u32[]{:S(2)}, u32[]{:S(2)}) collective-permute-start(bf16[16,128]{1,0:T(8,128)(2,1)S(1)} %get-tuple-element.44), channel_id=1, source_target_pairs={{0,4},{4,8},{8,12},{12,16},{16,20},{20,24},{24,28},{28,32},{32,36}... | collective-permute-start | bytes 12296 | tf_op jit(solution)/shard_map/ppermute | solution.py:350
  8.2 24.6 %all-to-all-start = ((bf16[64,8,128]{2,1,0:T(8,128)(2,1)}), bf16[64,8,128]{2,1,0:T(8,128)(2,1)S(1)}, u32[]{:S(2)}, u32[]{:S(2)}) async-start(bf16[64,8,128]{2,1,0:T(8,128)(2,1)} %get-tuple-element.45), calls=%async_computation | async-start | bytes 262144 | tf_op jit(solution)/shard_map/all_to_all | solution.py:299
  33.5 7.1 %collective-permute-start.1 = (bf16[32,2048]{1,0:T(8,128)(2,1)S(1)}, bf16[32,2048]{1,0:T(8,128)(2,1)S(1)}, u32[]{:S(2)}, u32[]{:S(2)}) collective-permute-start(bf16[32,2048]{1,0:T(8,128)(2,1)S(1)} %get-tuple-element.53), channel_id=1, source_target_pairs={{0,1},{1,2},{2,3},{3,0},{4,5},{5,6},{6,7},{7,4},{8,9},{9,10},{10,1... | collective-permute-start | bytes 393224 | tf_op jit(solution)/shard_map/ppermute | solution.py:295
  34.9 5.8 %collective-permute-start.2 = (bf16[32,2048]{1,0:T(8,128)(2,1)S(1)}, bf16[32,2048]{1,0:T(8,128)(2,1)S(1)}, u32[]{:S(2)}, u32[]{:S(2)}) collective-permute-start(bf16[32,2048]{1,0:T(8,128)(2,1)S(1)} %get-tuple-element.54), channel_id=1, source_target_pairs={{0,3},{1,0},{2,1},{3,2},{4,7},{5,4},{6,5},{7,6},{8,11},{9,8},{10,9... | collective-permute-start | bytes 393224 | tf_op jit(solution)/shard_map/ppermute | solution.py:295
  36.4 7.1 %collective-permute-start.3 = (bf16[32,2048]{1,0:T(8,128)(2,1)S(1)}, bf16[32,2048]{1,0:T(8,128)(2,1)S(1)}, u32[]{:S(2)}, u32[]{:S(2)}) collective-permute-start(bf16[32,2048]{1,0:T(8,128)(2,1)S(1)} %get-tuple-element.55), channel_id=1, source_target_pairs={{0,2},{1,3},{2,0},{3,1},{4,6},{5,7},{6,4},{7,5},{8,10},{9,11},{10,... | collective-permute-start | bytes 393224 | tf_op jit(solution)/shard_map/ppermute | solution.py:295
  38.0 17.2 %collective-permute-start.4 = (bf16[2048,128]{1,0:T(8,128)(2,1)}, bf16[2048,128]{1,0:T(8,128)(2,1)}, u32[]{:S(2)}, u32[]{:S(2)}) collective-permute-start(bf16[2048,128]{1,0:T(8,128)(2,1)} %bitcast.17.g0), channel_id=1, source_target_pairs={{0,1},{1,2},{2,3},{3,0},{4,5},{5,6},{6,7},{7,4},{8,9},{9,10},{10,1... | collective-permute-start | bytes 1572872 | tf_op jit(solution)/shard_map/ppermute | solution.py:295
  38.4 16.9 %collective-permute-start.7 = (bf16[2048,128]{1,0:T(8,128)(2,1)}, bf16[2048,128]{1,0:T(8,128)(2,1)}, u32[]{:S(2)}, u32[]{:S(2)}) collective-permute-start(bf16[2048,128]{1,0:T(8,128)(2,1)} %bitcast.18.u0), channel_id=1, source_target_pairs={{0,3},{1,0},{2,1},{3,2},{4,7},{5,4},{6,5},{7,6},{8,11},{9,8},{10,9... | collective-permute-start | bytes 1572872 | tf_op jit(solution)/shard_map/ppermute | solution.py:295
  40.6 25.7 %collective-permute-start.10 = (bf16[128,2048]{1,0:T(8,128)(2,1)}, bf16[128,2048]{1,0:T(8,128)(2,1)S(1)}, u32[]{:S(2)}, u32[]{:S(2)}) collective-permute-start(bf16[128,2048]{1,0:T(8,128)(2,1)} %bitcast.19.d0), channel_id=1, source_target_pairs={{0,1},{1,2},{2,3},{3,0},{4,5},{5,6},{6,7},{7,4},{8,9},{9,10},{10,1... | collective-permute-start | bytes 1572872 | tf_op jit(solution)/shard_map/ppermute | solution.py:295
  44.9 44.7 %all-to-all-start.1 = ((bf16[64,2,2048]{2,1,0:T(2,128)(2,1)}), bf16[64,2,2048]{2,1,0:T(2,128)(2,1)S(1)}, u32[]{:S(2)}, u32[]{:S(2)}) async-start(bf16[64,2,2048]{2,1,0:T(2,128)(2,1)} %get-tuple-element.60), calls=%async_computation.1 | async-start | bytes 1048576 | tf_op jit(solution)/shard_map/all_to_all | solution.py:299
  51.1 16.0 %collective-permute-start.11 = (bf16[128,2048]{1,0:T(8,128)(2,1)}, bf16[128,2048]{1,0:T(8,128)(2,1)S(1)}, u32[]{:S(2)}, u32[]{:S(2)}) collective-permute-start(bf16[128,2048]{1,0:T(8,128)(2,1)} %bitcast.19.d0), channel_id=1, source_target_pairs={{0,3},{1,0},{2,1},{3,2},{4,7},{5,4},{6,5},{7,6},{8,11},{9,8},{10,9... | collective-permute-start | bytes 1572872 | tf_op jit(solution)/shard_map/ppermute | solution.py:295
  52.4 25.2 %collective-permute-start.5 = (bf16[2048,128]{1,0:T(8,128)(2,1)}, bf16[2048,128]{1,0:T(8,128)(2,1)S(1)}, u32[]{:S(2)}, u32[]{:S(2)}) collective-permute-start(bf16[2048,128]{1,0:T(8,128)(2,1)} %bitcast.18.u0), channel_id=1, source_target_pairs={{0,1},{1,2},{2,3},{3,0},{4,5},{5,6},{6,7},{7,4},{8,9},{9,10},{10,1... | collective-permute-start | bytes 1572872 | tf_op jit(solution)/shard_map/ppermute | solution.py:295
  55.2 27.4 %collective-permute-start.6 = (bf16[2048,128]{1,0:T(8,128)(2,1)}, bf16[2048,128]{1,0:T(8,128)(2,1)S(1)}, u32[]{:S(2)}, u32[]{:S(2)}) collective-permute-start(bf16[2048,128]{1,0:T(8,128)(2,1)} %bitcast.17.g0), channel_id=1, source_target_pairs={{0,3},{1,0},{2,1},{3,2},{4,7},{5,4},{6,5},{7,6},{8,11},{9,8},{10,9... | collective-permute-start | bytes 1572872 | tf_op jit(solution)/shard_map/ppermute | solution.py:295
  55.2 33.6 %collective-permute-start.8 = (bf16[2048,128]{1,0:T(8,128)(2,1)}, bf16[2048,128]{1,0:T(8,128)(2,1)S(1)}, u32[]{:S(2)}, u32[]{:S(2)}) collective-permute-start(bf16[2048,128]{1,0:T(8,128)(2,1)} %collective-permute-done.4.g1), channel_id=1, source_target_pairs={{0,1},{1,2},{2,3},{3,0},{4,5},{5,6},{6,7},{7,4},{8,9},{9,10},{10,1... | collective-permute-start | bytes 1572872 | tf_op jit(solution)/shard_map/ppermute | solution.py:295
  66.3 0.8 copy-start
  66.3 23.3 %collective-permute-start.9 = (bf16[2048,128]{1,0:T(8,128)(2,1)}, bf16[2048,128]{1,0:T(8,128)(2,1)}, u32[]{:S(2)}, u32[]{:S(2)}) collective-permute-start(bf16[2048,128]{1,0:T(8,128)(2,1)} %collective-permute-done.7.u2), channel_id=1, source_target_pairs={{0,3},{1,0},{2,1},{3,2},{4,7},{5,4},{6,5},{7,6},{8,11},{9,8},{10,9... | collective-permute-start | bytes 1572872 | tf_op jit(solution)/shard_map/ppermute | solution.py:295
  67.1 10.4 %copy-start.1 = (bf16[128,2048]{1,0:T(8,128)(2,1)}, bf16[128,2048]{1,0:T(8,128)(2,1)S(1)}, u32[]{:S(2)}) copy-start(bf16[128,2048]{1,0:T(8,128)(2,1)S(1)} %collective-permute-done.11.d2) | copy-start | bytes 1572868
  67.1 27.3 %collective-permute-start.12 = (bf16[64,2048]{1,0:T(8,128)(2,1)S(1)}, bf16[64,2048]{1,0:T(8,128)(2,1)S(1)}, u32[]{:S(2)}, u32[]{:S(2)}) collective-permute-start(bf16[64,2048]{1,0:T(8,128)(2,1)S(1)} %slice.8), channel_id=1, source_target_pairs={{0,1},{1,2},{2,3},{3,0},{4,5},{5,6},{6,7},{7,4},{8,9},{9,10},{10,1... | collective-permute-start | bytes 786440 | tf_op jit(solution)/shard_map/ppermute | solution.py:295
  77.6 0.8 copy-start.2
  77.6 16.9 %collective-permute-start.13 = (bf16[64,2048]{1,0:T(8,128)(2,1)}, bf16[64,2048]{1,0:T(8,128)(2,1)S(1)}, u32[]{:S(2)}, u32[]{:S(2)}) collective-permute-start(bf16[64,2048]{1,0:T(8,128)(2,1)} %slice.9), channel_id=1, source_target_pairs={{0,3},{1,0},{2,1},{3,2},{4,7},{5,4},{6,5},{7,6},{8,11},{9,8},{10,9... | collective-permute-start | bytes 786440 | tf_op jit(solution)/shard_map/ppermute | solution.py:295
  82.7 6.1 %copy-start.3 = (bf16[2048,128]{1,0:T(8,128)(2,1)}, bf16[2048,128]{1,0:T(8,128)(2,1)S(1)}, u32[]{:S(2)}) copy-start(bf16[2048,128]{1,0:T(8,128)(2,1)S(1)} %collective-permute-done.6.g2) | copy-start | bytes 1572868
  88.8 0.8 copy-start.4
